TPU v7x, 32 devices: a whole 2x2x4 slice. The times are simulated.
32 devices in a mesh: rep: 2 (over x), fs: 8 (over z, y), tp: 2 (over core).
Axes of the slice: x: 2, y: 2, z: 4, core: 2. Of those that a mesh axis runs over, the one named last changes fastest.
Arguments:
- tokens: bfloat16 [5120, 2048], P(('rep', 'fs')), may hold values from -6 to 6
- gate_weight: float32 [2048, 5120], P('fs', 'tp'), may hold values from -0.125 to 0.125
- up_weight: float32 [2048, 5120], P('fs', 'tp'), may hold values from -0.125 to 0.125
- down_weight: float32 [2048, 5120], P('fs', 'tp'), may hold values from -0.078125 to 0.078125
- value_weight: float32 [2048, 2048], P('fs', 'tp'), may hold values from -0.125 to 0.125
- glu_weight: float32 [2048, 2048], P('fs', 'tp'), may hold values from -0.125 to 0.125
- out_weight: float32 [2048, 2048], P('fs', 'tp'), may hold values from -0.125 to 0.125
- gate_scale: float32 [5120], P('tp'), may hold values from 0.1 to 1.9
- up_scale: float32 [5120], P('tp'), may hold values from 0.5 to 2
- down_scale: float32 [2048], P('fs'), may hold values from 1 to 4
- value_scale: float32 [2048], P('tp'), may hold values from 0.2 to 3.4
- glu_scale: float32 [2048], P('tp'), may hold values from 0.1 to 1.9
- out_scale: float32 [2048], P('fs'), may hold values from 1 to 4
- conv_kernel: float32 [31, 2048], P(None, 'tp'), may hold values from -1 to 1
- norm_gain: float32 [2048], P('tp'), may hold values from 0.1 to 1.9
- first_gain: float32 [2048], replicated, may hold values from 0.1 to 1.9
- conv_gain: float32 [2048], replicated, may hold values from 0.1 to 1.9
- second_gain: float32 [2048], replicated, may hold values from 0.1 to 1.9
Outputs:
- result: bfloat16 [5120, 2048], P(('rep', 'fs'))
All inputs are finite; a program needn't handle non-finite values.
Results may differ from a plain program's by a relative error of at most 0.02.
Values may be sent and summed in bfloat16 or wider, within the bound.
A program may use at most 128 MiB of HBM per device.

v0:
```python
import jax
import jax.numpy as jnp
from jax import lax
from jax.sharding import PartitionSpec as P

D = 2048


EPSILON = 1e-06


def rms_rows(rows, gains):
    values = rows.astype(jnp.float32)
    scaled = values * lax.rsqrt(jnp.mean(values * values, axis=-1, keepdims=True) + EPSILON)
    return (scaled * gains).astype(jnp.bfloat16)


def gated_hidden(normed, gate_full, up_full, gate_scale, up_scale):
    gate_part = jnp.dot(normed, gate_full, preferred_element_type=jnp.float32) * gate_scale
    upward = jnp.dot(normed, up_full, preferred_element_type=jnp.float32) * up_scale
    return (jax.nn.silu(gate_part) * upward).astype(jnp.bfloat16)


def causal_depthwise(inputs, kernel):
    taps = kernel.shape[0]
    length = inputs.shape[0]
    padded = jnp.concatenate(
        [jnp.zeros((taps - 1, inputs.shape[1]), jnp.float32), inputs.astype(jnp.float32)], axis=0
    )
    total = jnp.zeros((length, inputs.shape[1]), jnp.float32)
    for offset in range(taps):
        total = total + kernel[offset] * padded[offset : offset + length]
    return total


def swap(values, axis):
    return lax.ppermute(values, axis, [(0, 1), (1, 0)])


def gather_rows(rows, axis):
    if lax.axis_size(axis) != 2:
        return lax.all_gather(rows, axis, axis=0, tiled=True)
    other = swap(rows, axis)
    first = lax.axis_index(axis) == 0
    return jnp.concatenate([jnp.where(first, rows, other), jnp.where(first, other, rows)], axis=0)


def scatter_rows(partial, axis):
    members = lax.axis_size(axis)
    if members != 2:
        return lax.psum_scatter(partial, axis, scatter_dimension=0, tiled=True).astype(jnp.float32)
    own_rows = partial.shape[0] // members
    place = lax.axis_index(axis)
    mine = lax.dynamic_slice_in_dim(partial, place * own_rows, own_rows, 0)
    theirs = lax.dynamic_slice_in_dim(partial, (1 - place) * own_rows, own_rows, 0)
    return mine.astype(jnp.float32) + swap(theirs, axis).astype(jnp.float32)


def pull(rows, step):
    n = lax.axis_size("rep")
    return lax.ppermute(rows, "rep", [(s, (s - step) % n) for s in range(n)])


def push(rows, step):
    n = lax.axis_size("rep")
    return lax.ppermute(rows, "rep", [(s, (s + step) % n) for s in range(n)])


def streams_of(own):
    n = lax.axis_size("rep")
    parts = [own] + [pull(own, step) for step in range(1, n)]
    return [gather_rows(part, "tp") for part in parts]


def owned_sum(actives, weight_rows):
    n = lax.axis_size("rep")
    total = None
    for step in list(range(1, n)) + [0]:
        partial = lax.dot_general(
            actives[step], weight_rows, (((1,), (1,)), ((), ())), preferred_element_type=jnp.float32
        ).astype(jnp.bfloat16)
        part = scatter_rows(partial, "tp")
        if step:
            part = push(part.astype(jnp.bfloat16), step).astype(jnp.float32)
        total = part if total is None else total + part
    return total


def local(
    tokens,
    gate_weight,
    up_weight,
    down_weight,
    value_weight,
    glu_weight,
    out_weight,
    gate_scale,
    up_scale,
    down_scale,
    value_scale,
    glu_scale,
    out_scale,
    conv_kernel,
    norm_gain,
    first_gain,
    conv_gain,
    second_gain,
):
    reps = lax.axis_size("rep")
    rep = lax.axis_index("rep")

    def part(array, dim):
        width = array.shape[dim] // reps
        return lax.dynamic_slice_in_dim(array, rep * width, width, dim)

    scales = lax.all_gather(jnp.stack([down_scale, out_scale]), "fs", axis=1, tiled=True)
    down_rows, out_rows = scales[0], scales[1]

    def full(weight):
        return lax.all_gather(part(weight, 1).astype(jnp.bfloat16), "fs", axis=0, tiled=True)

    gate_full, up_full, down_full, value_full, glu_full, out_full = (
        full(gate_weight),
        full(up_weight),
        full(down_weight),
        full(value_weight),
        full(glu_weight),
        full(out_weight),
    )
    gate_scale, up_scale, value_scale, glu_scale, norm_gain = (
        part(gate_scale, 0),
        part(up_scale, 0),
        part(value_scale, 0),
        part(glu_scale, 0),
        part(norm_gain, 0),
    )
    conv_kernel = part(conv_kernel, 1)
    members = lax.axis_size("tp")
    own_rows = tokens.shape[0] // members
    own_tokens = lax.dynamic_slice_in_dim(tokens, lax.axis_index("tp") * own_rows, own_rows, 0)

    normed = rms_rows(tokens, first_gain)
    own_normed = rms_rows(own_tokens, first_gain)
    rows = [normed] + [gather_rows(pull(own_normed, step), "tp") for step in range(1, reps)]
    hidden = [gated_hidden(r, gate_full, up_full, gate_scale, up_scale) for r in rows]
    after_first = (
        own_tokens.astype(jnp.float32) + 0.5 * down_rows * owned_sum(hidden, down_full)
    ).astype(jnp.bfloat16)
    mixes, sums = [], []
    for rows in streams_of(rms_rows(after_first, conv_gain)):
        value_part = jnp.dot(rows, value_full, preferred_element_type=jnp.float32) * value_scale
        gate_part = jnp.dot(rows, glu_full, preferred_element_type=jnp.float32) * glu_scale
        glu_in = (value_part * jax.nn.sigmoid(gate_part)).astype(jnp.bfloat16)
        mixed = causal_depthwise(glu_in, conv_kernel)
        mixes.append(mixed)
        sums.append(jnp.stack([jnp.sum(mixed, axis=1), jnp.sum(mixed * mixed, axis=1)]))
    totals = lax.psum(jnp.roll(jnp.stack(sums), rep, axis=0), ("rep", "tp"))
    totals = jnp.roll(totals, -rep, axis=0) / D
    actives = []
    for step, mixed in enumerate(mixes):
        mean_rows = totals[step, 0][:, None]
        square_rows = totals[step, 1][:, None]
        normalized = (
            (mixed - mean_rows) * lax.rsqrt(square_rows - mean_rows * mean_rows + EPSILON) * norm_gain
        )
        actives.append(jax.nn.silu(normalized).astype(jnp.bfloat16))
    after_conv = (after_first.astype(jnp.float32) + out_rows * owned_sum(actives, out_full)).astype(
        jnp.bfloat16
    )
    hidden = [
        gated_hidden(r, gate_full, up_full, gate_scale, up_scale)
        for r in streams_of(rms_rows(after_conv, second_gain))
    ]
    after_second = (
        after_conv.astype(jnp.float32) + 0.5 * down_rows * owned_sum(hidden, down_full)
    ).astype(jnp.bfloat16)
    return gather_rows(after_second, "tp")


def solution(mesh):
    placed = (
        P(("rep", "fs"), None),
        P("fs", "tp"),
        P("fs", "tp"),
        P("fs", "tp"),
        P("fs", "tp"),
        P("fs", "tp"),
        P("fs", "tp"),
        P("tp"),
        P("tp"),
        P("fs"),
        P("tp"),
        P("tp"),
        P("fs"),
        P(None, "tp"),
        P("tp"),
        P(),
        P(),
        P(),
    )
    return jax.shard_map(
        local, mesh=mesh, in_specs=placed, out_specs=P(("rep", "fs"), None), check_vma=False
    )
```

profile of v0, /device:TPU:0, one launch (start us, length us, event | category | flops | bytes accessed | tf_op | source)
XLA Modules:
  0.0 515.1 jit_solution(11567098746282541957)
XLA Ops:
  6.5 1.7 copy-done
  9.3 2.2 dynamic-slice_convert_fusion
  11.6 2.4 dynamic-slice_convert_fusion.1
  14.0 1.8 dynamic-slice_convert_fusion.4
  16.4 3.0 collective-permute-start
  19.4 14.7 %collective-permute-done = bf16[160,2048]{1,0:T(8,128)(2,1)S(1)} collective-permute-done((bf16[160,2048]{1,0:T(8,128)(2,1)S(1)}, bf16[160,2048]{1,0:T(8,128)(2,1)S(1)}, u32[]{:S(2)}, u32[]{:S(2)}) %collective-permute-start) | collective-permute-done | bytes 655392 | tf_op jit(solution)/shard_map/ppermute | solution.py:61
  34.1 1.8 dynamic-slice_convert_fusion.5
  36.5 1.0 broadcast_select_fusion.11
  37.5 60.7 %all-gather.7.cloned.1.call-done = bf16[2048,1280]{1,0:T(8,128)(2,1)} async-done(((bf16[256,1280]{1,0:T(8,128)(2,1)}), bf16[2048,1280]{1,0:T(8,128)(2,1)}) %all-gather.7.cloned.1.call-update) | async-done | bytes 5242896 | tf_op jit(solution)/shard_map/all_gather | solution.py:120
  98.2 5.8 %convolution_multiply_fusion.7 = f32[320,1280]{1,0:T(8,128)} fusion(bf16[2048,1280]{1,0:T(8,128)(2,1)} %all-gather.7.cloned.1.call-done, bf16[160,2048]{1,0:T(8,128)(2,1)} %get-tuple-element.31, bf16[160,2048]{1,0:T(8,128)(2,1)S(1)} %get-tuple-element.30, f32[1280]{0:T(1024)S(1)} %dynamic_slice.80), kind=kOutput, calls=%fused_computation.13 | convolution fusion | flops 1680752640 | bytes 8197120 | tf_op jit(solution)/shard_map/dot_general | solution.py:19
  103.9 80.5 %all-gather.11.cloned.1.call-done = bf16[2048,1280]{1,0:T(8,128)(2,1)} async-done(((bf16[256,1280]{1,0:T(8,128)(2,1)}), bf16[2048,1280]{1,0:T(8,128)(2,1)}) %all-gather.11.cloned.1.call-update) | async-done | bytes 5242896 | tf_op jit(solution)/shard_map/all_gather | solution.py:120
  184.4 86.3 %all-gather.9.cloned.1.call-done = bf16[2048,1280]{1,0:T(8,128)(2,1)} async-done(((bf16[256,1280]{1,0:T(8,128)(2,1)}), bf16[2048,1280]{1,0:T(8,128)(2,1)}) %all-gather.9.cloned.1.call-update) | async-done | bytes 5242896 | tf_op jit(solution)/shard_map/all_gather | solution.py:120
  270.7 8.8 %convolution_convert_fusion.3 = bf16[320,2048]{1,0:T(8,128)(2,1)S(1)} fusion(bf16[2048,1280]{1,0:T(8,128)(2,1)} %all-gather.11.cloned.1.call-done, bf16[2048,1280]{1,0:T(8,128)(2,1)} %all-gather.9.cloned.1.call-done, f32[320,1280]{1,0:T(8,128)} %convolution_multiply_fusion.7, bf16[160,2048]{1,0:T(8,128)(2,1)S(1)} %copy-done.9, ...), kind=kOutput, calls=%fused_computation.21 | convolution fusion | flops 3361587200 | bytes 14750720 | tf_op jit(solution)/shard_map/dot_general | solution.py:79
  279.6 1.0 constant_dynamic-slice_fusion.6
  280.8 5.6 %convolution_multiply_fusion.5 = f32[320,1280]{1,0:T(8,128)} fusion(bf16[2048,1280]{1,0:T(8,128)(2,1)} %all-gather.7.cloned.1.call-done, f32[1280]{0:T(1024)S(1)} %dynamic_slice.80, bf16[320,2048]{1,0:T(8,128)(2,1)S(1)} %copy-done.2, f32[2048]{0:T(1024)S(1)} %copy-done.13, f32[320]{0:T(512)S(1)} %add_rsqrt_fusion.2), kind=kOutput, calls=%fused_computation.10 | convolution fusion | flops 1680752640 | bytes 8206592 | tf_op jit(solution)/shard_map/dot_general | solution.py:19
  286.4 8.7 %convolution_convert_fusion.2 = bf16[320,2048]{1,0:T(8,128)(2,1)S(1)} fusion(bf16[2048,1280]{1,0:T(8,128)(2,1)} %all-gather.11.cloned.1.call-done, bf16[2048,1280]{1,0:T(8,128)(2,1)} %all-gather.9.cloned.1.call-done, f32[320,1280]{1,0:T(8,128)} %convolution_multiply_fusion.5, f32[1280]{0:T(1024)S(1)} %dynamic_slice.82, bf16[320,2048]{1,0:T(8,128)(2,1)S(1)} %copy-done.2, ...), kind=kOutput, calls=%fused_computation.20 | convolution fusion | flops 3361587200 | bytes 14760192 | tf_op jit(solution)/shard_map/dot_general | solution.py:79
  296.6 1.5 collective-permute-start.3
  298.2 26.7 %all_gather.21 = f32[2,2048]{1,0:T(2,128)S(1)} all-gather(f32[2,256]{1,0:T(2,128)S(1)} %pad_maximum_fusion.22), channel_id=1, replica_groups=mesh['rep'=2,'fs'=8,'tp'=2] {'fs'}, dimensions={1}, use_global_device_ids=true | all-gather | bytes 18432 | tf_op jit(solution)/shard_map/all_gather | solution.py:116
  326.5 1.8 dynamic-slice_convert_fusion.3
  328.6 1.2 fusion.192
  329.8 1.4 constant_dynamic-slice_fusion
  331.2 8.0 %collective-permute-done.5 = bf16[160,2048]{1,0:T(8,128)(2,1)S(1)} collective-permute-done((bf16[160,2048]{1,0:T(8,128)(2,1)S(1)}, bf16[160,2048]{1,0:T(8,128)(2,1)S(1)}, u32[]{:S(2)}, u32[]{:S(2)}) %collective-permute-start.5) | collective-permute-done | bytes 655392 | tf_op jit(solution)/shard_map/ppermute | solution.py:61
  339.2 1.3 broadcast_select_fusion.7
  340.5 3.7 fusion.26
  344.1 25.9 %all-gather.13.cloned.1.call-done = bf16[2048,512]{1,0:T(8,128)(2,1)} async-done(((bf16[256,512]{1,0:T(8,128)(2,1)}), bf16[2048,512]{1,0:T(8,128)(2,1)}) %all-gather.13.cloned.1.call-update) | async-done | bytes 2097168 | tf_op jit(solution)/shard_map/all_gather | solution.py:120
  370.0 2.6 fusion.36
  372.6 3.2 fusion.189
  375.9 1.4 copy-done.21
  377.4 0.9 fusion.31
  379.9 3.2 fusion.188
  383.2 6.4 %psum.7 = f32[2,2,320]{2,1,0:T(2,128)S(1)} all-reduce(f32[2,2,320]{2,1,0:T(2,128)S(1)} %fusion.167), channel_id=1, replica_groups=mesh['rep'=2,'fs'=8,'tp'=2] {'rep','tp'}, use_global_device_ids=true, to_apply=%region_7.9 | all-reduce | flops 1280 | bytes 10240 | tf_op jit(solution)/shard_map/psum | solution.py:157
  389.7 30.0 %all-gather.17.cloned.1.call-done = bf16[2048,512]{1,0:T(8,128)(2,1)} async-done(((bf16[256,512]{1,0:T(8,128)(2,1)}), bf16[2048,512]{1,0:T(8,128)(2,1)}) %all-gather.17.cloned.1.call-update) | async-done | bytes 2097168 | tf_op jit(solution)/shard_map/all_gather | solution.py:120
  419.6 2.7 convolution_convert_fusion.5
  422.6 1.0 convolution_convert_fusion.4
  424.8 1.5 collective-permute-start.9
  426.4 15.3 %collective-permute-done.9 = bf16[160,2048]{1,0:T(8,128)(2,1)S(1)} collective-permute-done((bf16[160,2048]{1,0:T(8,128)(2,1)S(1)}, bf16[160,2048]{1,0:T(8,128)(2,1)S(1)}, u32[]{:S(2)}, u32[]{:S(2)}) %collective-permute-start.9) | collective-permute-done | bytes 655392 | tf_op jit(solution)/shard_map/ppermute | solution.py:66
  442.6 1.5 collective-permute-start.11
  444.1 14.5 %collective-permute-done.11 = bf16[160,2048]{1,0:T(8,128)(2,1)S(1)} collective-permute-done((bf16[160,2048]{1,0:T(8,128)(2,1)S(1)}, bf16[160,2048]{1,0:T(8,128)(2,1)S(1)}, u32[]{:S(2)}, u32[]{:S(2)}) %collective-permute-start.11) | collective-permute-done | bytes 655392 | tf_op jit(solution)/shard_map/ppermute | solution.py:61
  459.1 3.1 convolution_multiply_fusion.1
  462.3 3.1 convolution_multiply_fusion.3
  465.4 8.6 %convolution_convert_fusion.1 = bf16[320,2048]{1,0:T(8,128)(2,1)S(1)} fusion(bf16[2048,1280]{1,0:T(8,128)(2,1)} %all-gather.11.cloned.1.call-done, bf16[2048,1280]{1,0:T(8,128)(2,1)} %all-gather.9.cloned.1.call-done, f32[320,1280]{1,0:T(8,128)} %convolution_multiply_fusion.3, bf16[160,2048]{1,0:T(8,128)(2,1)S(1)} %get-tuple-element.23, ...), kind=kOutput, calls=%fused_computation.19 | convolution fusion | flops 3361587200 | bytes 14750720 | tf_op jit(solution)/shard_map/dot_general | solution.py:79
  474.6 10.1 %convolution_convert_fusion = bf16[320,2048]{1,0:T(8,128)(2,1)} fusion(bf16[2048,1280]{1,0:T(8,128)(2,1)} %all-gather.11.cloned.1.call-done, bf16[2048,1280]{1,0:T(8,128)(2,1)} %all-gather.9.cloned.1.call-done, f32[320,1280]{1,0:T(8,128)} %convolution_multiply_fusion.1, bf16[160,2048]{1,0:T(8,128)(2,1)} %copy-done.7, bf16[160,2048]{1,0:T(8,128)(2,1)} %copy-done.6, ...), kind=kOutput, calls=%fused_computation.18 | convolution fusion | flops 3361587200 | bytes 14750720 | tf_op jit(solution)/shard_map/dot_general | solution.py:79
  484.7 1.2 constant_dynamic-slice_fusion.1
  486.2 1.5 collective-permute-start.14
  488.1 15.3 %collective-permute-done.14 = bf16[160,2048]{1,0:T(8,128)(2,1)S(1)} collective-permute-done((bf16[160,2048]{1,0:T(8,128)(2,1)S(1)}, bf16[160,2048]{1,0:T(8,128)(2,1)S(1)}, u32[]{:S(2)}, u32[]{:S(2)}) %collective-permute-start.14) | collective-permute-done | bytes 655392 | tf_op jit(solution)/shard_map/ppermute | solution.py:66
  504.0 2.1 collective-permute-done.17
  506.1 1.1 pad_maximum_fusion.5
  507.3 1.0 copy-done.1
  (130 shorter events, 12.3 us)
Async XLA Ops:
  6.5 1.7 copy-start
  6.5 91.6 %all-gather.7.cloned.1.call-start = ((), (), s32[]{:S(2)}) async-start(), calls=%async_computation | async-start | bytes 5898240 | tf_op jit(solution)/shard_map/all_gather | solution.py:120
  9.2 175.2 %all-gather.11.cloned.1.call-start = ((), (), s32[]{:S(2)}) async-start(), calls=%async_computation.2 | async-start | bytes 5898240 | tf_op jit(solution)/shard_map/all_gather | solution.py:120
  11.5 4.4 copy-start.2
  11.5 4.6 copy-start.13
  11.5 259.2 %all-gather.9.cloned.1.call-start = ((), (), s32[]{:S(2)}) async-start(), calls=%async_computation.1 | async-start | bytes 5898240 | tf_op jit(solution)/shard_map/all_gather | solution.py:120
  14.0 326.5 %all-gather.15.cloned.1.call-start = ((), (), s32[]{:S(2)}) async-start(), calls=%async_computation.4 | async-start | bytes 2359296 | tf_op jit(solution)/shard_map/all_gather | solution.py:120
  15.8 20.2 %copy-start.14 = (f32[2560]{0:T(1024)S(1)}, f32[2560]{0:T(1024)}, u32[]{:S(2)}) copy-start(f32[2560]{0:T(1024)} %param.27) | copy-start | bytes 30724
  15.8 20.3 %copy-start.15 = (f32[2560]{0:T(1024)S(1)}, f32[2560]{0:T(1024)}, u32[]{:S(2)}) copy-start(f32[2560]{0:T(1024)} %param.28) | copy-start | bytes 30724
  15.8 354.2 %all-gather.13.cloned.1.call-start = ((), (), s32[]{:S(2)}) async-start(), calls=%async_computation.3 | async-start | bytes 2359296 | tf_op jit(solution)/shard_map/all_gather | solution.py:120
  16.4 17.8 %collective-permute-start = (bf16[160,2048]{1,0:T(8,128)(2,1)S(1)}, bf16[160,2048]{1,0:T(8,128)(2,1)S(1)}, u32[]{:S(2)}, u32[]{:S(2)}) collective-permute-start(bf16[160,2048]{1,0:T(8,128)(2,1)S(1)} %fusion.13), channel_id=1, source_target_pairs={{0,16},{16,0},{1,17},{17,1},{2,18},{18,2},{3,19},{19,3},{4,20},{20... | collective-permute-start | bytes 1966088 | tf_op jit(solution)/shard_map/ppermute | solution.py:61
  34.1 2.4 collective-permute-start.1
  35.9 383.7 %all-gather.17.cloned.1.call-start = ((), (), s32[]{:S(2)}) async-start(), calls=%async_computation.5 | async-start | bytes 2359296 | tf_op jit(solution)/shard_map/all_gather | solution.py:120
  37.5 66.5 %copy-start.8 = (bf16[160,2048]{1,0:T(8,128)(2,1)}, bf16[160,2048]{1,0:T(8,128)(2,1)S(1)}, u32[]{:S(2)}) copy-start(bf16[160,2048]{1,0:T(8,128)(2,1)S(1)} %get-tuple-element.30) | copy-start | bytes 1966084
  98.2 172.6 %copy-start.9 = (bf16[160,2048]{1,0:T(8,128)(2,1)S(1)}, bf16[160,2048]{1,0:T(8,128)(2,1)}, u32[]{:S(2)}) copy-start(bf16[160,2048]{1,0:T(8,128)(2,1)} %get-tuple-element.31) | copy-start | bytes 1966084
  279.6 1.3 copy-start.3
  280.6 14.9 %collective-permute-start.2 = (bf16[160,2048]{1,0:T(8,128)(2,1)}, bf16[160,2048]{1,0:T(8,128)(2,1)S(1)}, u32[]{:S(2)}, u32[]{:S(2)}) collective-permute-start(bf16[160,2048]{1,0:T(8,128)(2,1)} %constant_dynamic-slice_fusion.6), channel_id=1, source_target_pairs={{0,1},{1,0},{2,3},{3,2},{4,5},{5,4},{6,7},{7,6},{8,9},{9,8},{10,11... | collective-permute-start | bytes 1966088 | tf_op jit(solution)/shard_map/ppermute | solution.py:37
  295.1 1.3 copy-start.4
  295.1 3.0 copy-start.19
  295.1 3.0 copy-start.20
  295.2 29.7 %collective-permute-start.4 = (bf16[160,2048]{1,0:T(8,128)(2,1)S(1)}, bf16[160,2048]{1,0:T(8,128)(2,1)S(1)}, u32[]{:S(2)}, u32[]{:S(2)}) collective-permute-start(bf16[160,2048]{1,0:T(8,128)(2,1)S(1)} %constant_dynamic-slice_fusion.5), channel_id=1, source_target_pairs={{0,1},{1,0},{2,3},{3,2},{4,5},{5,4},{6,7},{7,6},{8,9},{9,8},{10,11... | collective-permute-start | bytes 1966088 | tf_op jit(solution)/shard_map/ppermute | solution.py:37
  296.6 28.3 %collective-permute-start.3 = (bf16[160,2048]{1,0:T(8,128)(2,1)S(1)}, bf16[160,2048]{1,0:T(8,128)(2,1)S(1)}, u32[]{:S(2)}, u32[]{:S(2)}) collective-permute-start(bf16[160,2048]{1,0:T(8,128)(2,1)S(1)} %add_convert_fusion.2), channel_id=1, source_target_pairs={{0,16},{16,0},{1,17},{17,1},{2,18},{18,2},{3,19},{19,3},{4,20},{20... | collective-permute-start | bytes 1966088 | tf_op jit(solution)/shard_map/ppermute | solution.py:66
  325.5 2.8 copy-start.16
  325.5 2.9 copy-start.17
  325.5 2.9 copy-start.18
  325.9 13.3 %collective-permute-start.5 = (bf16[160,2048]{1,0:T(8,128)(2,1)S(1)}, bf16[160,2048]{1,0:T(8,128)(2,1)S(1)}, u32[]{:S(2)}, u32[]{:S(2)}) collective-permute-start(bf16[160,2048]{1,0:T(8,128)(2,1)S(1)} %fusion.17), channel_id=1, source_target_pairs={{0,16},{16,0},{1,17},{17,1},{2,18},{18,2},{3,19},{19,3},{4,20},{20... | collective-permute-start | bytes 1966088 | tf_op jit(solution)/shard_map/ppermute | solution.py:61
  326.5 12.7 %collective-permute-start.7 = (bf16[160,2048]{1,0:T(8,128)(2,1)S(1)}, bf16[160,2048]{1,0:T(8,128)(2,1)S(1)}, u32[]{:S(2)}, u32[]{:S(2)}) collective-permute-start(bf16[160,2048]{1,0:T(8,128)(2,1)S(1)} %fusion.17), channel_id=1, source_target_pairs={{0,1},{1,0},{2,3},{3,2},{4,5},{5,4},{6,7},{7,6},{8,9},{9,8},{10,11... | collective-permute-start | bytes 1966088 | tf_op jit(solution)/shard_map/ppermute | solution.py:37
  339.2 36.6 %collective-permute-start.6 = (bf16[160,2048]{1,0:T(8,128)(2,1)S(1)}, bf16[160,2048]{1,0:T(8,128)(2,1)S(1)}, u32[]{:S(2)}, u32[]{:S(2)}) collective-permute-start(bf16[160,2048]{1,0:T(8,128)(2,1)S(1)} %collective-permute-done.5), channel_id=1, source_target_pairs={{0,1},{1,0},{2,3},{3,2},{4,5},{5,4},{6,7},{7,6},{8,9},{9,8},{10,11... | collective-permute-start | bytes 1966088 | tf_op jit(solution)/shard_map/ppermute | solution.py:37
  340.5 29.5 %copy-start.10 = (bf16[160,2048]{1,0:T(8,128)(2,1)S(1)}, bf16[160,2048]{1,0:T(8,128)(2,1)}, u32[]{:S(2)}) copy-start(bf16[160,2048]{1,0:T(8,128)(2,1)} %get-tuple-element.29) | copy-start | bytes 1966084
  375.8 1.6 copy-start.21
  377.4 1.7 copy-start.22
  419.6 2.9 copy-start.23
  419.6 39.4 %slice-start = ((s8[5242880]{0:T(1024)(128)(4,1)}), s8[4194304]{0:T(1024)(128)(4,1)S(1)}, s32[]{:S(2)}) async-start(s8[5242880]{0:T(1024)(128)(4,1)} %bitcast.124), calls=%async_computation.6 | async-start | bytes 8388608
  422.4 2.2 collective-permute-start.8
  422.5 36.5 %slice-start.1 = ((s8[5242880]{0:T(1024)(128)(4,1)}), s8[1048576]{0:T(1024)(128)(4,1)S(1)}, s32[]{:S(2)}) async-start(s8[5242880]{0:T(1024)(128)(4,1)} %bitcast.124), calls=%async_computation.7 | async-start | bytes 2097152
  423.6 2.8 collective-permute-start.10
  424.8 16.8 %collective-permute-start.9 = (bf16[160,2048]{1,0:T(8,128)(2,1)S(1)}, bf16[160,2048]{1,0:T(8,128)(2,1)S(1)}, u32[]{:S(2)}, u32[]{:S(2)}) collective-permute-start(bf16[160,2048]{1,0:T(8,128)(2,1)S(1)} %add_convert_fusion.1), channel_id=1, source_target_pairs={{0,16},{16,0},{1,17},{17,1},{2,18},{18,2},{3,19},{19,3},{4,20},{20... | collective-permute-start | bytes 1966088 | tf_op jit(solution)/shard_map/ppermute | solution.py:66
  442.6 16.0 %collective-permute-start.11 = (bf16[160,2048]{1,0:T(8,128)(2,1)S(1)}, bf16[160,2048]{1,0:T(8,128)(2,1)S(1)}, u32[]{:S(2)}, u32[]{:S(2)}) collective-permute-start(bf16[160,2048]{1,0:T(8,128)(2,1)S(1)} %fusion.21), channel_id=1, source_target_pairs={{0,16},{16,0},{1,17},{17,1},{2,18},{18,2},{3,19},{19,3},{4,20},{20... | collective-permute-start | bytes 1966088 | tf_op jit(solution)/shard_map/ppermute | solution.py:61
  444.1 14.5 %collective-permute-start.15 = (bf16[160,2048]{1,0:T(8,128)(2,1)S(1)}, bf16[160,2048]{1,0:T(8,128)(2,1)S(1)}, u32[]{:S(2)}, u32[]{:S(2)}) collective-permute-start(bf16[160,2048]{1,0:T(8,128)(2,1)S(1)} %fusion.21), channel_id=1, source_target_pairs={{0,1},{1,0},{2,3},{3,2},{4,5},{5,4},{6,7},{7,6},{8,9},{9,8},{10,11... | collective-permute-start | bytes 1966088 | tf_op jit(solution)/shard_map/ppermute | solution.py:37
  458.6 3.6 collective-permute-start.12
  459.0 3.1 copy-start.6
  459.0 3.1 copy-start.7
  474.1 12.0 %collective-permute-start.13 = (bf16[160,2048]{1,0:T(8,128)(2,1)S(1)}, bf16[160,2048]{1,0:T(8,128)(2,1)S(1)}, u32[]{:S(2)}, u32[]{:S(2)}) collective-permute-start(bf16[160,2048]{1,0:T(8,128)(2,1)S(1)} %constant_dynamic-slice_fusion.2), channel_id=1, source_target_pairs={{0,1},{1,0},{2,3},{3,2},{4,5},{5,4},{6,7},{7,6},{8,9},{9,8},{10,11... | collective-permute-start | bytes 1966088 | tf_op jit(solution)/shard_map/ppermute | solution.py:37
  484.7 18.7 %copy-start.5 = (bf16[320,2048]{1,0:T(8,128)(2,1)S(1)}, bf16[320,2048]{1,0:T(8,128)(2,1)}, u32[]{:S(2)}) copy-start(bf16[320,2048]{1,0:T(8,128)(2,1)} %convolution_convert_fusion) | copy-start | bytes 3932164
  485.9 2.2 collective-permute-start.16
  486.2 17.2 %collective-permute-start.14 = (bf16[160,2048]{1,0:T(8,128)(2,1)S(1)}, bf16[160,2048]{1,0:T(8,128)(2,1)S(1)}, u32[]{:S(2)}, u32[]{:S(2)}) collective-permute-start(bf16[160,2048]{1,0:T(8,128)(2,1)S(1)} %add_convert_fusion), channel_id=1, source_target_pairs={{0,16},{16,0},{1,17},{17,1},{2,18},{18,2},{3,19},{19,3},{4,20},{20... | collective-permute-start | bytes 1966088 | tf_op jit(solution)/shard_map/ppermute | solution.py:66
  503.9 2.2 collective-permute-start.17
  506.0 2.2 copy-start.1
  (2 other events, 1.4 us)
Sparse Core Ops, SparseCore 0:
  9.5 88.5 all-gather.6
  100.3 84.0 all-gather.10
  186.6 84.0 all-gather.8
  272.7 47.4 all-gather.14
  322.2 47.7 all-gather.12
  372.0 47.6 all-gather.16
where the time goes:
time: 516 us; the launch traced here: 515 us
  waiting for transfers between devices  354 us (69%)
  matrix products  65.4 us (13%)
  blocking collectives  33.1 us (6%)
  local copies, waits for them, and re-layouts  22.6 us (4%)
  other arithmetic  14.1 us (3%)
  between operations  14.1 us (3%)
  starting transfers between devices  11.7 us (2%)
    all_gather x6, waiting for transfers between devices, full(): lax.all_gather(part(weight, 1).astype(jnp.bfloat16), 'fs', axis=0, tiled=...  283 us
    dot_general x6, matrix products, owned_sum(): lax.dot_general(actives[step], weight_rows, (((1,), (1,)), ((), ())), pre...  39.9 us
    ppermute x3, waiting for transfers between devices, pull(): return lax.ppermute(rows, 'rep', [(s, (s - step) % n) for s in range(n)])  37.2 us
    ppermute x3, waiting for transfers between devices, push(): return lax.ppermute(rows, 'rep', [(s, (s + step) % n) for s in range(n)])  30.6 us
    all_gather x1, blocking collectives, local(): lax.all_gather(jnp.stack([down_scale, out_scale]), 'fs', axis=1, tiled=True)  26.7 us
    dot_general x4, matrix products, gated_hidden(): jnp.dot(normed, gate_full, preferred_element_type=jnp.float32) * gate_scale  17.5 us
    convert_element_type x6, local copies, waits for them, and re-layouts, full(): part(weight, 1).astype(jnp.bfloat16)  10.8 us
  transfers between devices with their start and end apart: 24, of which 13 were waited for; matrix products, arithmetic and copies ran while one was open for 15% of the time, Pallas kernels for 0%

commit v1 on v0

--- a/solution.py
+++ b/solution.py
@@ -1,12 +1,461 @@
+import functools
+
 import jax
 import jax.numpy as jnp
 from jax import lax
+from jax.experimental import pallas as pl
+from jax.experimental.pallas import tpu as pltpu
 from jax.sharding import PartitionSpec as P
 
-D = 2048
-
-
+MESH = pl.DeviceIdType.MESH
 EPSILON = 1e-06
+LANES = 128
+TILE = 256
+ROWS = 16
+NT = (((1,), (1,)), ((), ()))
+TN = (((0,), (0,)), ((), ()))
+
+
+def fused_kernel(dims, *refs):
+    S, D, H, C, KW, F, RX = dims
+    Z = F // 2
+    SH = S // 2
+    R = 2 * RX
+    PAD = -(-(KW - 1) // 8) * 8
+    (tokens, m0, m1, m2, m3, t0, t1, t2, t3, sc_in, first_gain, conv_gain, second_gain, gate_scale, up_scale,
+     value_scale, glu_scale, norm_gain, conv_k, out, *scratch) = refs
+    (wb0, wb1, wb2, wb3, tokv, xa, xb, xc, hid, part, rc, ry, ys, res, gp, mixed, act, st, scl, dsc,
+     loc_sem, y_send, y_recv, u_send, d_send, z_recv, x_send, x_recv, tok_sem, s_send, s_recv,
+     rc_send, rc_recv, ry_send, ry_recv, ag_send, ag_recv, st_send, st_recv, out_sem) = scratch
+    mine, theirs, wb = (m0, m1, m2, m3), (t0, t1, t2, t3), (wb0, wb1, wb2, wb3)
+    G = len(wb)
+
+    x = lax.axis_index("rep")
+    f = lax.axis_index("fs")
+    c = lax.axis_index("tp")
+    y = lax.rem(f, 2)
+    z = lax.div(f, 2)
+    fp = f + 1 - 2 * y
+    ox, oy, oc = 1 - x, 1 - y, 1 - c
+    dx, dc, dy, dyc = {"rep": ox}, {"tp": oc}, {"fs": fp}, {"fs": fp, "tp": oc}
+    up, dn = {"fs": f + 2}, {"fs": f - 2}
+
+    def rcopy(src, dst, ssem, rsem, dev):
+        return pltpu.make_async_remote_copy(
+            src_ref=src, dst_ref=dst, send_sem=ssem, recv_sem=rsem, device_id=dev, device_id_type=MESH
+        )
+
+    barrier = pltpu.get_barrier_semaphore()
+    for j in range(1, F):
+        pl.semaphore_signal(barrier, inc=1, device_id={"fs": lax.rem(f + j, F)}, device_id_type=MESH)
+    for dev in (dx, dc, dyc):
+        pl.semaphore_signal(barrier, inc=1, device_id=dev, device_id_type=MESH)
+    pl.semaphore_wait(barrier, F + 2)
+
+    def y_copy(g, h):
+        return rcopy(theirs[g].at[h], wb[g].at[2 * f + h], y_send.at[g, h], y_recv.at[g, h], dy)
+
+    def y_wait(g, h):
+        b = wb[g].at[2 * fp + h]
+        rcopy(b, b, y_send.at[g, h], y_recv.at[g, h], dy).wait_recv()
+
+    def z_copy(g, q, sems, dev, own=False):
+        b = wb[g].at[2 * q + x]
+        return rcopy(mine[g].at[x] if own else b, b, sems.at[g, q], z_recv.at[g, q], dev)
+
+    def x_copy(g, q):
+        b = wb[g].at[2 * q + x]
+        return rcopy(b, b, x_send.at[g, q], x_recv.at[g, q], dx)
+
+    def local_copy(g):
+        return pltpu.make_async_copy(mine[g], wb[g].at[pl.ds(2 * f, 2)], loc_sem.at[g])
+
+    def send_own(g):
+        @pl.when(z < Z - 1)
+        def _():
+            z_copy(g, f, u_send, up, True).start()
+
+        @pl.when(z > 0)
+        def _():
+            z_copy(g, f, d_send, dn, True).start()
+
+    def send_pair(g):
+        y_wait(g, x)
+
+        @pl.when(z < Z - 1)
+        def _():
+            z_copy(g, fp, u_send, up).start()
+
+        @pl.when(z > 0)
+        def _():
+            z_copy(g, fp, d_send, dn).start()
+
+    def forward(g, d):
+        for k in range(2):
+            yy = y if k == 0 else oy
+
+            @pl.when(z >= d)
+            def _():
+                q = 2 * (z - d) + yy
+                z_copy(g, q, u_send, up).wait_recv()
+
+                @pl.when(z < Z - 1)
+                def _():
+                    z_copy(g, q, u_send, up).start()
+
+                x_copy(g, q).start()
+
+            @pl.when(z + d < Z)
+            def _():
+                q = 2 * (z + d) + yy
+                z_copy(g, q, d_send, dn).wait_recv()
+
+                @pl.when(z > 0)
+                def _():
+                    z_copy(g, q, d_send, dn).start()
+
+                x_copy(g, q).start()
+
+    def group_done(g):
+        local_copy(g).wait()
+        y_wait(g, ox)
+        for d in range(1, Z):
+            for yy in range(2):
+                for side in (-1, 1):
+                    @pl.when((z >= d) if side < 0 else (z + d < Z))
+                    def _():
+                        q = 2 * (z + side * d) + yy
+                        b = wb[g].at[2 * q + ox]
+                        rcopy(b, b, x_send.at[g, q], x_recv.at[g, q], dx).wait_recv()
+
+    def drain(g):
+        for h in range(2):
+            y_copy(g, h).wait_send()
+        for q in range(F):
+            zq = q // 2
+
+            @pl.when((z < Z - 1) & (zq <= z))
+            def _():
+                z_copy(g, q, u_send, up).wait_send()
+
+            @pl.when((z > 0) & (zq >= z))
+            def _():
+                z_copy(g, q, d_send, dn).wait_send()
+
+            @pl.when(zq != z)
+            def _():
+                x_copy(g, q).wait_send()
+
+    y_copy(0, x).start()
+    send_own(0)
+    tok_local = pltpu.make_async_copy(tokens, tokv.at[y], out_sem.at[2])
+    tok_local.start()
+    for g in range(1, G):
+        y_copy(g, x).start()
+    for g in range(G):
+        local_copy(g).start()
+    y_copy(0, ox).start()
+    tok_y = rcopy(tokens, tokv.at[y], tok_sem.at[0], tok_sem.at[1], dy)
+    tok_y.start()
+    for g in range(1, G):
+        y_copy(g, ox).start()
+    own_scale = pltpu.make_async_copy(sc_in, scl.at[f], out_sem.at[3])
+    own_scale.start()
+    for j in range(1, F):
+        rcopy(sc_in, scl.at[f], s_send.at[j], s_recv.at[f], {"fs": lax.rem(f + j, F)}).start()
+
+    def norm(v, gains):
+        return (v * lax.rsqrt(jnp.mean(v * v, axis=-1, keepdims=True) + EPSILON) * gains).astype(jnp.bfloat16)
+
+    def norm_tokens(s):
+        @pl.loop(0, S // ROWS)
+        def _(i):
+            r = pl.ds(i * ROWS, ROWS)
+            xa[s, r, :] = norm(tokv[s, r, :].astype(jnp.float32), first_gain[...])
+
+    def gate_up(src, s):
+        @pl.loop(0, H // TILE)
+        def _(j):
+            lo = pl.multiple_of(j * TILE, TILE)
+            a = src[s]
+            gw = wb0[:, :, pl.ds(lo, TILE)].reshape(D, TILE)
+            uw = wb0[:, :, pl.ds(H + lo, TILE)].reshape(D, TILE)
+            gv = jnp.dot(a, gw, preferred_element_type=jnp.float32) * gate_scale[:, pl.ds(lo, TILE)]
+            uv = jnp.dot(a, uw, preferred_element_type=jnp.float32) * up_scale[:, pl.ds(lo, TILE)]
+            hid[s, :, pl.ds(lo, TILE)] = (gv * jax.nn.sigmoid(gv) * uv).astype(jnp.bfloat16)
+
+    def project(src, w, width, s):
+        @pl.loop(0, F)
+        def _(j):
+            rows = w[pl.ds(2 * j, 2)].reshape(R, width)
+            p = lax.dot_general(src[s], rows, NT, preferred_element_type=jnp.float32)
+            part[s, :, pl.ds(pl.multiple_of(j * R, R), R)] = p.astype(jnp.bfloat16)
+
+    crows = pl.ds(c * SH, SH)
+    orows = pl.ds(oc * SH, SH)
+
+    def rs_core(u, s):
+        return rcopy(part.at[s, orows], rc.at[u, s], rc_send.at[u, s], rc_recv.at[u, s], dc)
+
+    def rs_pair(u):
+        return rcopy(ys.at[u], ry.at[u], ry_send.at[u], ry_recv.at[u], dy)
+
+    def rs_push(u):
+        rs_core(u, oy).wait_recv()
+
+        @pl.loop(0, SH // ROWS)
+        def _(i):
+            r = pl.ds(i * ROWS, ROWS)
+            p = part[oy, pl.ds(c * SH + i * ROWS, ROWS), :].astype(jnp.float32)
+            ys[u, r, :] = (p + rc[u, oy, r, :].astype(jnp.float32)).astype(jnp.bfloat16)
+
+        rs_pair(u).start()
+
+    def rs_finish(u, base, factor, scale_row, gains, dst):
+        rs_core(u, y).wait_recv()
+        rs_pair(u).wait_recv()
+        sc = dsc[scale_row:scale_row + 1, :] * factor
+
+        @pl.loop(0, SH // ROWS)
+        def _(i):
+            r = pl.ds(i * ROWS, ROWS)
+            rr = pl.ds(c * SH + i * ROWS, ROWS)
+            total = part[y, rr, :].astype(jnp.float32) + rc[u, y, r, :].astype(jnp.float32)
+            total = total + ry[u, r, :].astype(jnp.float32)
+            b = tokv[y, rr, :] if base is None else res[base, r, :]
+            now = (b.astype(jnp.float32) + sc * total).astype(jnp.bfloat16)
+            res[u, r, :] = now
+            if dst is not None:
+                dst[y, rr, :] = norm(now.astype(jnp.float32), gains[...])
+
+    def ag_core(u, buf):
+        b = buf.at[y, crows]
+        return rcopy(b, b, ag_send.at[u, 0], ag_recv.at[u, 0], dc)
+
+    def ag_pair(u, buf):
+        b = buf.at[y, crows]
+        return rcopy(b, b, ag_send.at[u, 1], ag_recv.at[u, 1], dy)
+
+    def ag_relay(u, buf):
+        b = buf.at[oy, crows]
+        return rcopy(b, b, ag_send.at[u, 2], ag_recv.at[u, 2], dc)
+
+    def ag_wait(u, k, buf, s, rows):
+        b = buf.at[s, rows]
+        rcopy(b, b, ag_send.at[u, k], ag_recv.at[u, k], dc).wait_recv()
+
+    def ag_start(u, buf):
+        ag_pair(u, buf).start()
+        ag_core(u, buf).start()
+
+    def ag_pass(u, buf):
+        ag_wait(u, 1, buf, oy, crows)
+        ag_relay(u, buf).start()
+        ag_wait(u, 0, buf, y, orows)
+
+    def value_glu(s):
+        @pl.loop(0, C // TILE)
+        def _(j):
+            lo = pl.multiple_of(j * TILE, TILE)
+            a = xb[s]
+            vw = wb2[:, :, pl.ds(lo, TILE)].reshape(D, TILE)
+            gw = wb2[:, :, pl.ds(C + lo, TILE)].reshape(D, TILE)
+            vv = jnp.dot(a, vw, preferred_element_type=jnp.float32) * value_scale[:, pl.ds(lo, TILE)]
+            gv = jnp.dot(a, gw, preferred_element_type=jnp.float32) * glu_scale[:, pl.ds(lo, TILE)]
+            g = (vv * jax.nn.sigmoid(gv)).astype(jnp.bfloat16)
+            gp[s, pl.ds(PAD, S), pl.ds(lo, TILE)] = g.astype(jnp.float32)
+
+    def convolve(s):
+        @pl.loop(0, C // LANES)
+        def _(j):
+            cols = pl.ds(pl.multiple_of(j * LANES, LANES), LANES)
+            gp[s, pl.ds(0, PAD), cols] = jnp.zeros((PAD, LANES), jnp.float32)
+            total = jnp.zeros((S, LANES), jnp.float32)
+            for k in range(KW):
+                total = total + conv_k[k:k + 1, cols] * gp[s, pl.ds(PAD - (KW - 1) + k, S), cols]
+            mixed[s, :, cols] = total
+
+        m = mixed[s]
+        low = lax.broadcasted_iota(jnp.int32, (8, C), 0) < 4
+        one, nil = jnp.ones((8, C), jnp.float32), jnp.zeros((8, C), jnp.float32)
+        hi = lax.Precision.HIGHEST
+        sums = lax.dot_general(jnp.where(low, one, nil), m, NT, precision=hi, preferred_element_type=jnp.float32)
+        squares = lax.dot_general(jnp.where(low, nil, one), m * m, NT, precision=hi, preferred_element_type=jnp.float32)
+        st[0, s] = sums + squares
+
+    def st_copies():
+        return [rcopy(st.at[0], st.at[k + 1], st_send.at[k], st_recv.at[k], dev) for k, dev in enumerate((dc, dy, dyc))]
+
+    def activate(s):
+        total = st[0, s] + st[1, s] + st[2, s] + st[3, s]
+        total = total / D
+        mean, square = total[0:1], total[4:5]
+        rstd = lax.rsqrt(square - mean * mean + EPSILON)
+        row = lax.broadcasted_iota(jnp.int32, (8, S), 0)
+        both = jnp.where(row == 0, jnp.broadcast_to(mean, (8, S)), jnp.where(row == 1, jnp.broadcast_to(rstd, (8, S)), 0.0))
+        pick = lax.broadcasted_iota(jnp.int32, (8, LANES), 0)
+        hi = lax.Precision.HIGHEST
+        mcol = lax.dot_general(both, jnp.where(pick == 0, 1.0, 0.0), TN, precision=hi, preferred_element_type=jnp.float32)
+        rcol = lax.dot_general(both, jnp.where(pick == 1, 1.0, 0.0), TN, precision=hi, preferred_element_type=jnp.float32)
+        for j in range(C // LANES):
+            cols = slice(j * LANES, (j + 1) * LANES)
+            v = (mixed[s, :, cols] - mcol) * rcol * norm_gain[:, cols]
+            act[s, :, cols] = (v * jax.nn.sigmoid(v)).astype(jnp.bfloat16)
+
+    def own_and_pair(g):
+        send_own(g)
+        send_pair(g)
+
+    send_pair(0)
+    tok_local.wait()
+    norm_tokens(y)
+    forward(0, 1)
+    for d in range(2, Z - 1):
+        forward(0, d)
+    own_and_pair(1)
+    tok_y.wait_recv()
+    norm_tokens(oy)
+    forward(0, Z - 1)
+    forward(1, 1)
+    group_done(0)
+    gate_up(xa, oy)
+    for d in range(2, Z - 1):
+        forward(1, d)
+    own_and_pair(2)
+    gate_up(xa, y)
+    forward(1, Z - 1)
+    forward(2, 1)
+    group_done(1)
+    project(hid, wb1, H, oy)
+    rs_core(0, oy).start()
+    project(hid, wb1, H, y)
+    rs_core(0, y).start()
+    rs_push(0)
+    own_scale.wait()
+    for j in range(1, F):
+        b = scl.at[lax.rem(f + j, F)]
+        rcopy(b, b, s_send.at[j], s_recv.at[lax.rem(f + j, F)], dy).wait_recv()
+    for j in range(F):
+        dsc[:, j * R:(j + 1) * R] = scl[j]
+    for d in range(2, Z - 1):
+        forward(2, d)
+    own_and_pair(3)
+    forward(2, Z - 1)
+    forward(3, 1)
+    rs_finish(0, None, 0.5, 0, conv_gain, xb)
+    ag_start(0, xb)
+    for d in range(2, Z):
+        forward(3, d)
+    ag_pass(0, xb)
+    group_done(2)
+    value_glu(y)
+    convolve(y)
+    ag_wait(0, 2, xb, oy, orows)
+    value_glu(oy)
+    convolve(oy)
+    for cp in st_copies():
+        cp.start()
+    for s in range(2):
+        rs_core(0, s).wait_send()
+    for cp in st_copies():
+        cp.wait()
+    group_done(3)
+    activate(oy)
+    project(act, wb3, C, oy)
+    rs_core(1, oy).start()
+    activate(y)
+    project(act, wb3, C, y)
+    rs_core(1, y).start()
+    rs_push(1)
+    rs_finish(1, 0, 1.0, 1, second_gain, xc)
+    ag_start(1, xc)
+    ag_pass(1, xc)
+    gate_up(xc, y)
+    for s in range(2):
+        rs_core(1, s).wait_send()
+    ag_wait(1, 2, xc, oy, orows)
+    gate_up(xc, oy)
+    project(hid, wb1, H, oy)
+    rs_core(2, oy).start()
+    project(hid, wb1, H, y)
+    rs_core(2, y).start()
+    rs_push(2)
+    rs_finish(2, 1, 0.5, 0, None, None)
+    out_local = pltpu.make_async_copy(res.at[2], out.at[crows], out_sem.at[0])
+    out_local.start()
+    out_core = rcopy(res.at[2], out.at[crows], tok_sem.at[2], out_sem.at[1], dc)
+    out_core.start()
+    for g in range(G):
+        drain(g)
+    tok_y.wait_send()
+    for j in range(1, F):
+        rcopy(sc_in, scl.at[f], s_send.at[j], s_recv.at[f], dy).wait_send()
+    for s in range(2):
+        rs_core(2, s).wait_send()
+    for u in range(3):
+        rs_pair(u).wait_send()
+    for u, buf in enumerate((xb, xc)):
+        ag_core(u, buf).wait_send()
+        ag_pair(u, buf).wait_send()
+        ag_relay(u, buf).wait_send()
+    out_local.wait()
+    out_core.wait_send()
+    b = out.at[orows]
+    rcopy(b, b, tok_sem.at[2], out_sem.at[1], dc).wait_recv()
+
+
+def local_fused(tokens, gate_weight, up_weight, down_weight, value_weight, glu_weight, out_weight, gate_scale, up_scale,
+                down_scale, value_scale, glu_scale, out_scale, conv_kernel, norm_gain, first_gain, conv_gain, second_gain):
+    F = lax.axis_size("fs")
+    S, D = tokens.shape
+    R, H = gate_weight.shape[0], gate_weight.shape[1] // 2
+    C = value_weight.shape[1] // 2
+    KW = conv_kernel.shape[0]
+    RX = R // 2
+    SH = S // 2
+    y = lax.rem(lax.axis_index("fs"), 2)
+
+    def part(array, side, dim):
+        width = array.shape[dim] // 2
+        return lax.dynamic_slice_in_dim(array, side * width, width, dim)
+
+    def pack(side, *weights):
+        cut = [part(w, side, 1).astype(jnp.bfloat16) for w in weights]
+        whole = cut[0] if len(cut) == 1 else jnp.concatenate(cut, axis=1)
+        return whole.reshape(2, RX, whole.shape[1])
+
+    groups = ((gate_weight, up_weight), (down_weight,), (value_weight, glu_weight), (out_weight,))
+    mine = [pack(y, *g) for g in groups]
+    theirs = [pack(1 - y, *g) for g in groups]
+    scales = jnp.zeros((8, R), jnp.float32).at[0].set(down_scale).at[1].set(out_scale)
+    rows = [v.reshape(1, -1) for v in (first_gain, conv_gain, second_gain)]
+    rows += [part(v, y, 0).reshape(1, -1) for v in (gate_scale, up_scale, value_scale, glu_scale, norm_gain)]
+    taps = part(conv_kernel, y, 1)
+    widths = [m.shape[2] for m in mine]
+    G = len(groups)
+    bf, f32 = jnp.bfloat16, jnp.float32
+    dma = pltpu.SemaphoreType.DMA
+    anyspace = pl.BlockSpec(memory_space=pl.ANY)
+    vmem = pl.BlockSpec(memory_space=pltpu.VMEM)
+    pad = -(-(KW - 1) // 8) * 8
+    return pl.pallas_call(
+        functools.partial(fused_kernel, (S, D, H, C, KW, F, RX)),
+        out_shape=jax.ShapeDtypeStruct((S, D), bf),
+        in_specs=[anyspace] * (2 + 2 * G) + [vmem] * 9,
+        out_specs=anyspace,
+        scratch_shapes=[pltpu.VMEM((2 * F, RX, w), bf) for w in widths]
+        + [pltpu.VMEM((2, S, D), bf)] * 4
+        + [pltpu.VMEM((2, S, H), bf), pltpu.VMEM((2, S, D), bf)]
+        + [pltpu.VMEM((3, 2, SH, D), bf), pltpu.VMEM((3, SH, D), bf), pltpu.VMEM((3, SH, D), bf), pltpu.VMEM((3, SH, D), bf)]
+        + [pltpu.VMEM((2, S + pad, C), f32), pltpu.VMEM((2, S, C), f32), pltpu.VMEM((2, S, C), bf)]
+        + [pltpu.VMEM((4, 2, 8, S), f32), pltpu.VMEM((F, 8, R), f32), pltpu.VMEM((8, D), f32)]
+        + [dma((G,)), dma((G, 2)), dma((G, 2)), dma((G, F)), dma((G, F)), dma((G, F)), dma((G, F)), dma((G, F))]
+        + [dma((3,)), dma((F,)), dma((F,))]
+        + [dma((3, 2)), dma((3, 2)), dma((3,)), dma((3,)), dma((2, 3)), dma((2, 3)), dma((3,)), dma((3,)), dma((4,))],
+        compiler_params=pltpu.CompilerParams(
+            collective_id=0, has_side_effects=True, vmem_limit_bytes=64 * 1024 * 1024 - 65536
+        ),
+    )(tokens, *mine, *theirs, scales, *rows, taps)
 
 
 def rms_rows(rows, gains):
@@ -86,7 +535,7 @@
     return total
 
 
-def local(
+def local_plain(
     tokens,
     gate_weight,
     up_weight,
@@ -155,7 +604,7 @@
         mixes.append(mixed)
         sums.append(jnp.stack([jnp.sum(mixed, axis=1), jnp.sum(mixed * mixed, axis=1)]))
     totals = lax.psum(jnp.roll(jnp.stack(sums), rep, axis=0), ("rep", "tp"))
-    totals = jnp.roll(totals, -rep, axis=0) / D
+    totals = jnp.roll(totals, -rep, axis=0) / (norm_gain.shape[0] * reps * lax.axis_size("tp"))
     actives = []
     for step, mixed in enumerate(mixes):
         mean_rows = totals[step, 0][:, None]
@@ -177,27 +626,12 @@
     return gather_rows(after_second, "tp")
 
 
+def fits(mesh):
+    return mesh.shape["rep"] == 2 and mesh.shape["tp"] == 2 and mesh.shape["fs"] % 2 == 0 and mesh.shape["fs"] >= 4
+
+
 def solution(mesh):
-    placed = (
-        P(("rep", "fs"), None),
-        P("fs", "tp"),
-        P("fs", "tp"),
-        P("fs", "tp"),
-        P("fs", "tp"),
-        P("fs", "tp"),
-        P("fs", "tp"),
-        P("tp"),
-        P("tp"),
-        P("fs"),
-        P("tp"),
-        P("tp"),
-        P("fs"),
-        P(None, "tp"),
-        P("tp"),
-        P(),
-        P(),
-        P(),
-    )
-    return jax.shard_map(
-        local, mesh=mesh, in_specs=placed, out_specs=P(("rep", "fs"), None), check_vma=False
-    )
+    columns, rows = P("fs", "tp"), P(("rep", "fs"), None)
+    placed = (rows,) + (columns,) * 6 + (P("tp"), P("tp"), P("fs"), P("tp"), P("tp"), P("fs"), P(None, "tp"), P("tp"), P(), P(), P())
+    local = local_fused if fits(mesh) else local_plain
+    return jax.shard_map(local, mesh=mesh, in_specs=placed, out_specs=rows, check_vma=False)

time: 516 us -> 307 us (0.59)
  waiting for transfers between devices: 354 us -> 0 us
  Pallas kernels: 0 us -> 285 us
  matrix products: 65.4 us -> 0 us
  blocking collectives: 33.1 us -> 0 us
  between operations: 14.1 us -> 0.05 us
  starting transfers between devices: 11.7 us -> 0 us
  other arithmetic: 14.1 us -> 4.02 us
    pallas_call x0 -> x1, Pallas kernels: none -> 285 us  [local_fused(): pl.pallas_call(functools.partial(fused_kernel, (S, D, H, C, KW, F, RX)),...]
    all_gather x6 -> x0, waiting for transfers between devices: 283 us -> none  [full(): lax.all_gather(part(weight, 1).astype(jnp.bfloat16), 'fs', axis=0, tiled=...]
    ppermute x18 -> x0, waiting for transfers between devices: 70.8 us -> none  [the longest x3 37.2 us: pull(): return lax.ppermute(rows, 'rep', [(s, (s - step) % n) for s in range(n)])]
    dot_general x14 -> x0, matrix products: 65.4 us -> none  [the longest x6 39.9 us: owned_sum(): lax.dot_general(actives[step], weight_rows, (((1,), (1,)), ((), ())), pre...]
    all_gather x1 -> x0, blocking collectives: 26.7 us -> none  [local(): lax.all_gather(jnp.stack([down_scale, out_scale]), 'fs', axis=1, tiled=True)]
    ppermute x18 -> x0, starting transfers between devices: 11.5 us -> none  [the longest x3 5.19 us: pull(): return lax.ppermute(rows, 'rep', [(s, (s - step) % n) for s in range(n)])]
    reduce_sum x6 -> x0, other arithmetic: 8.11 us -> none  [the longest x2 6.4 us: local(): jnp.sum(mixed, axis=1)]
    psum x1 -> x0, blocking collectives: 6.38 us -> none  [local(): totals = lax.psum(jnp.roll(jnp.stack(sums), rep, axis=0), ('rep', 'tp'))]
  transfers between devices with their start and end apart: 24 -> 0, of which waited for: 13 -> 0; matrix products, arithmetic and copies ran while one was open for 15% -> 0% of each run, Pallas kernels for 0% -> 0%
where the time goes in v1:
time: 307 us
  Pallas kernels  285 us (93%)
  local copies, waits for them, and re-layouts  17.9 us (6%)
  other arithmetic  4.02 us (1%)
    pallas_call x1, Pallas kernels, local_fused(): pl.pallas_call(functools.partial(fused_kernel, (S, D, H, C, KW, F, RX)),...  285 us
    dynamic_slice x6, local copies, waits for them, and re-layouts, part(): return lax.dynamic_slice_in_dim(array, side * width, width, dim)  7.05 us

profile of v1, /device:TPU:0, one launch (start us, length us, event | category | flops | bytes accessed | tf_op | source)
XLA Modules:
  0.0 306.8 jit_solution(12033958795433084340)
XLA Ops:
  0.0 1.3 dynamic_slice.68
  1.3 1.3 dynamic_slice.69
  2.7 1.3 dynamic_slice.70
  4.0 0.8 dynamic_slice.66
  4.8 0.6 reshape.113.refs_13_
  5.4 0.8 dynamic_slice.67
  6.2 0.6 reshape.114.refs_14_
  6.8 0.7 scatter.6
  7.5 0.7 scatter.9.refs_9_
  8.2 0.0 copy-start.3
  8.2 1.5 constant_dynamic-slice_fusion.refs_18_
  9.6 0.0 copy-start
  9.6 1.4 dynamic-slice_convert_fusion.8
  11.1 0.0 copy-start.2
  11.1 2.6 dynamic-slice_convert_fusion.6
  13.7 0.0 copy-start.1
  13.7 0.9 pad_maximum_fusion.2
  14.5 0.9 pad_maximum_fusion.3
  15.4 0.0 copy-done.3
  15.4 0.0 copy-done
  15.4 0.2 dynamic-slice_convert_fusion.2
  15.6 0.0 copy-done.2
  15.6 0.1 copy-done.1
  15.7 1.4 dynamic-slice_convert_fusion
  17.1 1.1 pad_maximum_fusion
  18.3 1.2 pad_maximum_fusion.1
  19.4 284.9 %shard_map.172 = bf16[320,2048]{1,0:T(8,128)(2,1)} custom-call(bf16[320,2048]{1,0:T(8,128)(2,1)} %refs_0_.1, bf16[2,128,2560]{2,1,0:T(8,128)(2,1)} %bitcast.16, bf16[2,128,1280]{2,1,0:T(8,128)(2,1)} %bitcast.19, bf16[2,128,1024]{2,1,0:T(8,128)(2,1)} %bitcast.20, bf16[2,128,512]{2,1,0:T(8,128)(2,1)} %bitcast.23, bf16[2,128,2560]{2,1,0:T(8,128)(2,1)} %bitcast.17, ...), custom_call_target="tpu_custom_call" | custom-call | tf_op jit(solution)/shard_map/pallas_call | solution.py:441
  304.3 2.5 copy.21
Async XLA Ops:
  8.2 7.2 %copy-start.3 = (f32[8,256]{1,0:T(8,128)}, f32[8,256]{1,0:T(8,128)S(1)}, u32[]{:S(2)}) copy-start(f32[8,256]{1,0:T(8,128)S(1)} %scatter.9.refs_9_) | copy-start | bytes 24580
  9.6 5.8 %copy-start = (f32[256,2560]{1,0:T(8,128)S(1)}, f32[256,2560]{1,0:T(8,128)}, u32[]{:S(2)}) copy-start(f32[256,2560]{1,0:T(8,128)} %param.23) | copy-start | bytes 7864324
  11.1 4.5 %copy-start.2 = (f32[256,2560]{1,0:T(8,128)S(1)}, f32[256,2560]{1,0:T(8,128)}, u32[]{:S(2)}) copy-start(f32[256,2560]{1,0:T(8,128)} %param.24) | copy-start | bytes 7864324
  13.7 2.0 copy-start.1

commit v2 on v1

--- a/solution.py
+++ b/solution.py
@@ -12,6 +12,9 @@
 LANES = 128
 TILE = 256
 ROWS = 16
+CHUNK = 32
+SUBS = (1, 1, 1, 1)
+COLS = 4
 NT = (((1,), (1,)), ((), ()))
 TN = (((0,), (0,)), ((), ()))
 
@@ -22,12 +25,14 @@
     SH = S // 2
     R = 2 * RX
     PAD = -(-(KW - 1) // 8) * 8
-    (tokens, m0, m1, m2, m3, t0, t1, t2, t3, sc_in, first_gain, conv_gain, second_gain, gate_scale, up_scale,
-     value_scale, glu_scale, norm_gain, conv_k, out, *scratch) = refs
-    (wb0, wb1, wb2, wb3, tokv, xa, xb, xc, hid, part, rc, ry, ys, res, gp, mixed, act, st, scl, dsc,
-     loc_sem, y_send, y_recv, u_send, d_send, z_recv, x_send, x_recv, tok_sem, s_send, s_recv,
-     rc_send, rc_recv, ry_send, ry_recv, ag_send, ag_recv, st_send, st_recv, out_sem) = scratch
-    mine, theirs, wb = (m0, m1, m2, m3), (t0, t1, t2, t3), (wb0, wb1, wb2, wb3)
+    K, DC = SH // CHUNK, D // COLS
+    (tokens, gate_w, up_w, down_w, value_w, glu_w, out_w, down_scale, out_scale, first_gain, conv_gain, second_gain,
+     gate_scale, up_scale, value_scale, glu_scale, norm_gain, conv_k, out, *scratch) = refs
+    (wb0, wb1, wb2, wb3, t0, t1, t2, t3, sg, tokv, xa, xb, xc, hid, part, rc, ry, ys, res, gp, mixed, act, st, sc, scl, dsc,
+     f_sem, y_send, y_recv, u_send, d_send, z_recv, x_send, x_recv, tok_sem, s_send, s_recv,
+     rc_send, rc_recv, ry_send, ry_recv, ag_send, ag_recv, fc_send, fc_recv, fy_send, fy_recv,
+     st_send, st_recv, out_sem, oc_send, oc_recv) = scratch
+    theirs, wb = (t0, t1, t2, t3), (wb0, wb1, wb2, wb3)
     G = len(wb)
 
     x = lax.axis_index("rep")
@@ -45,6 +50,35 @@
             src_ref=src, dst_ref=dst, send_sem=ssem, recv_sem=rsem, device_id=dev, device_id_type=MESH
         )
 
+    def fetch(slot, ref, width, h, k):
+        rows = pl.ds(h * RX, RX)
+        return pltpu.make_async_copy(ref.at[rows], sg.at[slot, rows, pl.ds(0, width)], f_sem.at[slot, k])
+
+    def fetch_start(slot, ref, width):
+        for k, h in enumerate((x, ox)):
+            fetch(slot, ref, width, h, k).start()
+
+    def round_rows(g, off, slot, ref, width, k):
+        h = (x, ox)[k]
+        fetch(slot, ref, 2 * width, h, k).wait()
+
+        @pl.loop(0, RX // ROWS)
+        def _(i):
+            rows = pl.ds(h * RX + i * ROWS, ROWS)
+            r = pl.ds(i * ROWS, ROWS)
+            near = sg[slot, rows, pl.ds(pl.multiple_of(y * width, LANES), width)]
+            far = sg[slot, rows, pl.ds(pl.multiple_of(oy * width, LANES), width)]
+            theirs[g][h, r, off:off + width] = far.astype(jnp.bfloat16)
+            wb[g][2 * f + h, r, off:off + width] = near.astype(jnp.bfloat16)
+
+    fetch_start(0, gate_w, 2 * H)
+    fetch_start(1, up_w, 2 * H)
+    tok_local = pltpu.make_async_copy(tokens, tokv.at[y], out_sem.at[0])
+    tok_local.start()
+    sc[...] = jnp.zeros_like(sc)
+    sc[0:1, :] = down_scale[...]
+    sc[1:2, :] = out_scale[...]
+
     barrier = pltpu.get_barrier_semaphore()
     for j in range(1, F):
         pl.semaphore_signal(barrier, inc=1, device_id={"fs": lax.rem(f + j, F)}, device_id_type=MESH)
@@ -52,117 +86,131 @@
         pl.semaphore_signal(barrier, inc=1, device_id=dev, device_id_type=MESH)
     pl.semaphore_wait(barrier, F + 2)
 
-    def y_copy(g, h):
-        return rcopy(theirs[g].at[h], wb[g].at[2 * f + h], y_send.at[g, h], y_recv.at[g, h], dy)
-
-    def y_wait(g, h):
-        b = wb[g].at[2 * fp + h]
-        rcopy(b, b, y_send.at[g, h], y_recv.at[g, h], dy).wait_recv()
-
-    def z_copy(g, q, sems, dev, own=False):
-        b = wb[g].at[2 * q + x]
-        return rcopy(mine[g].at[x] if own else b, b, sems.at[g, q], z_recv.at[g, q], dev)
-
-    def x_copy(g, q):
-        b = wb[g].at[2 * q + x]
-        return rcopy(b, b, x_send.at[g, q], x_recv.at[g, q], dx)
-
-    def local_copy(g):
-        return pltpu.make_async_copy(mine[g], wb[g].at[pl.ds(2 * f, 2)], loc_sem.at[g])
-
-    def send_own(g):
-        @pl.when(z < Z - 1)
-        def _():
-            z_copy(g, f, u_send, up, True).start()
-
-        @pl.when(z > 0)
-        def _():
-            z_copy(g, f, d_send, dn, True).start()
-
-    def send_pair(g):
-        y_wait(g, x)
-
-        @pl.when(z < Z - 1)
-        def _():
-            z_copy(g, fp, u_send, up).start()
-
-        @pl.when(z > 0)
-        def _():
-            z_copy(g, fp, d_send, dn).start()
+    def piece(g, ref, lead, i):
+        n = RX // SUBS[g]
+        return ref.at[lead, pl.ds(i * n, n)]
+
+    def y_copy(g, h, k, i):
+        return rcopy(piece(g, theirs[g], h, i), piece(g, wb[g], 2 * f + h, i), y_send.at[g, k, i], y_recv.at[g, k, i], dy)
+
+    def y_start(g, k):
+        for i in range(SUBS[g]):
+            y_copy(g, (x, ox)[k], k, i).start()
+
+    def y_wait(g, h, k, i):
+        b = piece(g, wb[g], 2 * fp + h, i)
+        rcopy(b, b, y_send.at[g, k, i], y_recv.at[g, k, i], dy).wait_recv()
+
+    def z_copy(g, q, i, sems, dev):
+        b = piece(g, wb[g], 2 * q + x, i)
+        return rcopy(b, b, sems.at[g, q, i], z_recv.at[g, q, i], dev)
+
+    def x_copy(g, q, i):
+        b = piece(g, wb[g], 2 * q + x, i)
+        return rcopy(b, b, x_send.at[g, q, i], x_recv.at[g, q, i], dx)
+
+    def send_rows(g, q, wait):
+        for i in range(SUBS[g]):
+            if wait:
+                y_wait(g, x, 0, i)
+
+            @pl.when(z < Z - 1)
+            def _():
+                z_copy(g, q, i, u_send, up).start()
+
+            @pl.when(z > 0)
+            def _():
+                z_copy(g, q, i, d_send, dn).start()
 
     def forward(g, d):
         for k in range(2):
             yy = y if k == 0 else oy
-
-            @pl.when(z >= d)
+            for i in range(SUBS[g]):
+                @pl.when(z >= d)
+                def _():
+                    q = 2 * (z - d) + yy
+                    z_copy(g, q, i, u_send, up).wait_recv()
+
+                    @pl.when(z < Z - 1)
+                    def _():
+                        z_copy(g, q, i, u_send, up).start()
+
+                    x_copy(g, q, i).start()
+
+                @pl.when(z + d < Z)
+                def _():
+                    q = 2 * (z + d) + yy
+                    z_copy(g, q, i, d_send, dn).wait_recv()
+
+                    @pl.when(z > 0)
+                    def _():
+                        z_copy(g, q, i, d_send, dn).start()
+
+                    x_copy(g, q, i).start()
+
+    def group_done(g):
+        for i in range(SUBS[g]):
+            y_wait(g, ox, 1, i)
+
+        @pl.loop(0, F)
+        def _(q):
+            @pl.when(lax.div(q, 2) != z)
             def _():
-                q = 2 * (z - d) + yy
-                z_copy(g, q, u_send, up).wait_recv()
-
-                @pl.when(z < Z - 1)
-                def _():
-                    z_copy(g, q, u_send, up).start()
-
-                x_copy(g, q).start()
-
-            @pl.when(z + d < Z)
-            def _():
-                q = 2 * (z + d) + yy
-                z_copy(g, q, d_send, dn).wait_recv()
-
-                @pl.when(z > 0)
-                def _():
-                    z_copy(g, q, d_send, dn).start()
-
-                x_copy(g, q).start()
-
-    def group_done(g):
-        local_copy(g).wait()
-        y_wait(g, ox)
-        for d in range(1, Z):
-            for yy in range(2):
-                for side in (-1, 1):
-                    @pl.when((z >= d) if side < 0 else (z + d < Z))
-                    def _():
-                        q = 2 * (z + side * d) + yy
-                        b = wb[g].at[2 * q + ox]
-                        rcopy(b, b, x_send.at[g, q], x_recv.at[g, q], dx).wait_recv()
+                for i in range(SUBS[g]):
+                    b = piece(g, wb[g], 2 * q + ox, i)
+                    rcopy(b, b, x_send.at[g, q, i], x_recv.at[g, q, i], dx).wait_recv()
 
     def drain(g):
-        for h in range(2):
-            y_copy(g, h).wait_send()
-        for q in range(F):
-            zq = q // 2
+        for k, h in enumerate((x, ox)):
+            for i in range(SUBS[g]):
+                y_copy(g, h, k, i).wait_send()
+
+        @pl.loop(0, F)
+        def _(q):
+            zq = lax.div(q, 2)
 
             @pl.when((z < Z - 1) & (zq <= z))
             def _():
-                z_copy(g, q, u_send, up).wait_send()
+                for i in range(SUBS[g]):
+                    z_copy(g, q, i, u_send, up).wait_send()
 
             @pl.when((z > 0) & (zq >= z))
             def _():
-                z_copy(g, q, d_send, dn).wait_send()
+                for i in range(SUBS[g]):
+                    z_copy(g, q, i, d_send, dn).wait_send()
 
             @pl.when(zq != z)
             def _():
-                x_copy(g, q).wait_send()
-
-    y_copy(0, x).start()
-    send_own(0)
-    tok_local = pltpu.make_async_copy(tokens, tokv.at[y], out_sem.at[2])
-    tok_local.start()
-    for g in range(1, G):
-        y_copy(g, x).start()
-    for g in range(G):
-        local_copy(g).start()
-    y_copy(0, ox).start()
+                for i in range(SUBS[g]):
+                    x_copy(g, q, i).wait_send()
+
+    for k in range(2):
+        round_rows(0, 0, 0, gate_w, H, k)
+        round_rows(0, H, 1, up_w, H, k)
+    y_start(0, 0)
+    send_rows(0, f, False)
+    fetch_start(0, down_w, 2 * H)
+    fetch_start(1, value_w, 2 * C)
+    for k in range(2):
+        round_rows(1, 0, 0, down_w, H, k)
+    fetch_start(0, glu_w, 2 * C)
+    y_start(1, 0)
+    for k in range(2):
+        round_rows(2, 0, 1, value_w, C, k)
+    fetch_start(1, out_w, 2 * C)
+    for k in range(2):
+        round_rows(2, C, 0, glu_w, C, k)
+    y_start(2, 0)
+    for k in range(2):
+        round_rows(3, 0, 1, out_w, C, k)
+    y_start(3, 0)
+    y_start(0, 1)
     tok_y = rcopy(tokens, tokv.at[y], tok_sem.at[0], tok_sem.at[1], dy)
     tok_y.start()
     for g in range(1, G):
-        y_copy(g, ox).start()
-    own_scale = pltpu.make_async_copy(sc_in, scl.at[f], out_sem.at[3])
-    own_scale.start()
+        y_start(g, 1)
     for j in range(1, F):
-        rcopy(sc_in, scl.at[f], s_send.at[j], s_recv.at[f], {"fs": lax.rem(f + j, F)}).start()
+        rcopy(sc, scl.at[f], s_send.at[j], s_recv.at[f], {"fs": lax.rem(f + j, F)}).start()
 
     def norm(v, gains):
         return (v * lax.rsqrt(jnp.mean(v * v, axis=-1, keepdims=True) + EPSILON) * gains).astype(jnp.bfloat16)
@@ -180,12 +228,12 @@
             a = src[s]
             gw = wb0[:, :, pl.ds(lo, TILE)].reshape(D, TILE)
             uw = wb0[:, :, pl.ds(H + lo, TILE)].reshape(D, TILE)
-            gv = jnp.dot(a, gw, preferred_element_type=jnp.float32) * gate_scale[:, pl.ds(lo, TILE)]
-            uv = jnp.dot(a, uw, preferred_element_type=jnp.float32) * up_scale[:, pl.ds(lo, TILE)]
+            gv = jnp.dot(a, gw, preferred_element_type=jnp.float32) * gate_scale[:, pl.ds(pl.multiple_of(y * H + lo, LANES), TILE)]
+            uv = jnp.dot(a, uw, preferred_element_type=jnp.float32) * up_scale[:, pl.ds(pl.multiple_of(y * H + lo, LANES), TILE)]
             hid[s, :, pl.ds(lo, TILE)] = (gv * jax.nn.sigmoid(gv) * uv).astype(jnp.bfloat16)
 
-    def project(src, w, width, s):
-        @pl.loop(0, F)
+    def project(src, w, width, s, first=0, last=F):
+        @pl.loop(first, last)
         def _(j):
             rows = w[pl.ds(2 * j, 2)].reshape(R, width)
             p = lax.dot_general(src[s], rows, NT, preferred_element_type=jnp.float32)
@@ -197,61 +245,103 @@
     def rs_core(u, s):
         return rcopy(part.at[s, orows], rc.at[u, s], rc_send.at[u, s], rc_recv.at[u, s], dc)
 
-    def rs_pair(u):
-        return rcopy(ys.at[u], ry.at[u], ry_send.at[u], ry_recv.at[u], dy)
+    def rs_pair(u, k):
+        r = pl.ds(k * CHUNK, CHUNK)
+        return rcopy(ys.at[u, r], ry.at[u, r], ry_send.at[u, k], ry_recv.at[u, k], dy)
 
     def rs_push(u):
         rs_core(u, oy).wait_recv()
+        for k in range(K):
+            @pl.loop(0, CHUNK // ROWS)
+            def _(i):
+                r = pl.ds(k * CHUNK + i * ROWS, ROWS)
+                p = part[oy, pl.ds(c * SH + k * CHUNK + i * ROWS, ROWS), :].astype(jnp.float32)
+                ys[u, r, :] = (p + rc[u, oy, r, :].astype(jnp.float32)).astype(jnp.bfloat16)
+
+            rs_pair(u, k).start()
+
+    def rs_finish(u, base, factor, scale_row, gains, dst):
+        rs_core(u, y).wait_recv()
+        for k in range(K):
+            rs_pair(u, k).wait_recv()
+
+            @pl.loop(0, CHUNK // ROWS)
+            def _(i):
+                r = pl.ds(k * CHUNK + i * ROWS, ROWS)
+                rr = pl.ds(c * SH + k * CHUNK + i * ROWS, ROWS)
+                total = part[y, rr, :].astype(jnp.float32) + rc[u, y, r, :].astype(jnp.float32)
+                total = total + ry[u, r, :].astype(jnp.float32)
+                b = tokv[y, rr, :] if base is None else res[base, r, :]
+                now = (b.astype(jnp.float32) + dsc[scale_row:scale_row + 1, :] * factor * total).astype(jnp.bfloat16)
+                res[u, r, :] = now
+                dst[y, rr, :] = norm(now.astype(jnp.float32), gains[...])
+
+            ag_copy(u, 1, k, dst).start()
+            ag_copy(u, 0, k, dst).start()
+
+    def ag_rows(k, side):
+        return pl.ds(side * SH + k * CHUNK, CHUNK)
+
+    def ag_copy(u, kind, k, buf):
+        b = buf.at[oy if kind == 2 else y, ag_rows(k, c)]
+        return rcopy(b, b, ag_send.at[u, kind, k], ag_recv.at[u, kind, k], dy if kind == 1 else dc)
+
+    def ag_wait(u, kind, k, buf):
+        b = buf.at[y if kind == 0 else oy, ag_rows(k, c if kind == 1 else oc)]
+        rcopy(b, b, ag_send.at[u, kind, k], ag_recv.at[u, kind, k], dc).wait_recv()
+
+    def ag_pass(u, buf, first, last):
+        for k in range(first, last):
+            ag_wait(u, 1, k, buf)
+            ag_copy(u, 2, k, buf).start()
+
+    def ag_own(u, buf):
+        for k in range(K):
+            ag_wait(u, 0, k, buf)
+
+    def ag_other(u, buf):
+        for k in range(K):
+            ag_wait(u, 2, k, buf)
+
+    def fc_copy(s, q):
+        cols = pl.ds(q * DC, DC)
+        return rcopy(part.at[s, orows, cols], rc.at[2, s, :, cols], fc_send.at[s, q], fc_recv.at[s, q], dc)
+
+    def fy_copy(q):
+        cols = pl.ds(q * DC, DC)
+        return rcopy(ys.at[2, :, cols], ry.at[2, :, cols], fy_send.at[q], fy_recv.at[q], dy)
+
+    def last_push(q):
+        cols = pl.ds(q * DC, DC)
+        fc_copy(oy, q).wait_recv()
 
         @pl.loop(0, SH // ROWS)
         def _(i):
             r = pl.ds(i * ROWS, ROWS)
-            p = part[oy, pl.ds(c * SH + i * ROWS, ROWS), :].astype(jnp.float32)
-            ys[u, r, :] = (p + rc[u, oy, r, :].astype(jnp.float32)).astype(jnp.bfloat16)
-
-        rs_pair(u).start()
-
-    def rs_finish(u, base, factor, scale_row, gains, dst):
-        rs_core(u, y).wait_recv()
-        rs_pair(u).wait_recv()
-        sc = dsc[scale_row:scale_row + 1, :] * factor
+            p = part[oy, pl.ds(c * SH + i * ROWS, ROWS), cols].astype(jnp.float32)
+            ys[2, r, cols] = (p + rc[2, oy, r, cols].astype(jnp.float32)).astype(jnp.bfloat16)
+
+        fy_copy(q).start()
+
+    def out_copies(q):
+        cols = pl.ds(q * DC, DC)
+        src, dst = res.at[2, :, cols], out.at[crows, cols]
+        return pltpu.make_async_copy(src, dst, out_sem.at[q]), rcopy(src, dst, oc_send.at[q], oc_recv.at[q], dc)
+
+    def last_finish(q):
+        cols = pl.ds(q * DC, DC)
+        fc_copy(y, q).wait_recv()
+        fy_copy(q).wait_recv()
 
         @pl.loop(0, SH // ROWS)
         def _(i):
             r = pl.ds(i * ROWS, ROWS)
-            rr = pl.ds(c * SH + i * ROWS, ROWS)
-            total = part[y, rr, :].astype(jnp.float32) + rc[u, y, r, :].astype(jnp.float32)
-            total = total + ry[u, r, :].astype(jnp.float32)
-            b = tokv[y, rr, :] if base is None else res[base, r, :]
-            now = (b.astype(jnp.float32) + sc * total).astype(jnp.bfloat16)
-            res[u, r, :] = now
-            if dst is not None:
-                dst[y, rr, :] = norm(now.astype(jnp.float32), gains[...])
-
-    def ag_core(u, buf):
-        b = buf.at[y, crows]
-        return rcopy(b, b, ag_send.at[u, 0], ag_recv.at[u, 0], dc)
-
-    def ag_pair(u, buf):
-        b = buf.at[y, crows]
-        return rcopy(b, b, ag_send.at[u, 1], ag_recv.at[u, 1], dy)
-
-    def ag_relay(u, buf):
-        b = buf.at[oy, crows]
-        return rcopy(b, b, ag_send.at[u, 2], ag_recv.at[u, 2], dc)
-
-    def ag_wait(u, k, buf, s, rows):
-        b = buf.at[s, rows]
-        rcopy(b, b, ag_send.at[u, k], ag_recv.at[u, k], dc).wait_recv()
-
-    def ag_start(u, buf):
-        ag_pair(u, buf).start()
-        ag_core(u, buf).start()
-
-    def ag_pass(u, buf):
-        ag_wait(u, 1, buf, oy, crows)
-        ag_relay(u, buf).start()
-        ag_wait(u, 0, buf, y, orows)
+            total = part[y, pl.ds(c * SH + i * ROWS, ROWS), cols].astype(jnp.float32) + rc[2, y, r, cols].astype(jnp.float32)
+            total = total + ry[2, r, cols].astype(jnp.float32)
+            res[2, r, cols] = (res[1, r, cols].astype(jnp.float32) + 0.5 * dsc[0:1, cols] * total).astype(jnp.bfloat16)
+
+        for cp in out_copies(q):
+            cp.start()
 
     def value_glu(s):
         @pl.loop(0, C // TILE)
@@ -260,8 +350,8 @@
             a = xb[s]
             vw = wb2[:, :, pl.ds(lo, TILE)].reshape(D, TILE)
             gw = wb2[:, :, pl.ds(C + lo, TILE)].reshape(D, TILE)
-            vv = jnp.dot(a, vw, preferred_element_type=jnp.float32) * value_scale[:, pl.ds(lo, TILE)]
-            gv = jnp.dot(a, gw, preferred_element_type=jnp.float32) * glu_scale[:, pl.ds(lo, TILE)]
+            vv = jnp.dot(a, vw, preferred_element_type=jnp.float32) * value_scale[:, pl.ds(pl.multiple_of(y * C + lo, LANES), TILE)]
+            gv = jnp.dot(a, gw, preferred_element_type=jnp.float32) * glu_scale[:, pl.ds(pl.multiple_of(y * C + lo, LANES), TILE)]
             g = (vv * jax.nn.sigmoid(gv)).astype(jnp.bfloat16)
             gp[s, pl.ds(PAD, S), pl.ds(lo, TILE)] = g.astype(jnp.float32)
 
@@ -269,10 +359,11 @@
         @pl.loop(0, C // LANES)
         def _(j):
             cols = pl.ds(pl.multiple_of(j * LANES, LANES), LANES)
+            near = pl.ds(pl.multiple_of(y * C + j * LANES, LANES), LANES)
             gp[s, pl.ds(0, PAD), cols] = jnp.zeros((PAD, LANES), jnp.float32)
             total = jnp.zeros((S, LANES), jnp.float32)
             for k in range(KW):
-                total = total + conv_k[k:k + 1, cols] * gp[s, pl.ds(PAD - (KW - 1) + k, S), cols]
+                total = total + conv_k[k:k + 1, near] * gp[s, pl.ds(PAD - (KW - 1) + k, S), cols]
             mixed[s, :, cols] = total
 
         m = mixed[s]
@@ -299,14 +390,14 @@
         rcol = lax.dot_general(both, jnp.where(pick == 1, 1.0, 0.0), TN, precision=hi, preferred_element_type=jnp.float32)
         for j in range(C // LANES):
             cols = slice(j * LANES, (j + 1) * LANES)
-            v = (mixed[s, :, cols] - mcol) * rcol * norm_gain[:, cols]
+            v = (mixed[s, :, cols] - mcol) * rcol * norm_gain[:, pl.ds(pl.multiple_of(y * C + j * LANES, LANES), LANES)]
             act[s, :, cols] = (v * jax.nn.sigmoid(v)).astype(jnp.bfloat16)
 
     def own_and_pair(g):
-        send_own(g)
-        send_pair(g)
-
-    send_pair(0)
+        send_rows(g, f, False)
+        send_rows(g, fp, True)
+
+    send_rows(0, fp, True)
     tok_local.wait()
     norm_tokens(y)
     forward(0, 1)
@@ -331,10 +422,10 @@
     project(hid, wb1, H, y)
     rs_core(0, y).start()
     rs_push(0)
-    own_scale.wait()
     for j in range(1, F):
         b = scl.at[lax.rem(f + j, F)]
         rcopy(b, b, s_send.at[j], s_recv.at[lax.rem(f + j, F)], dy).wait_recv()
+    scl[f] = sc[...]
     for j in range(F):
         dsc[:, j * R:(j + 1) * R] = scl[j]
     for d in range(2, Z - 1):
@@ -343,14 +434,14 @@
     forward(2, Z - 1)
     forward(3, 1)
     rs_finish(0, None, 0.5, 0, conv_gain, xb)
-    ag_start(0, xb)
     for d in range(2, Z):
         forward(3, d)
-    ag_pass(0, xb)
+    ag_pass(0, xb, 0, K)
+    ag_own(0, xb)
     group_done(2)
     value_glu(y)
     convolve(y)
-    ag_wait(0, 2, xb, oy, orows)
+    ag_other(0, xb)
     value_glu(oy)
     convolve(oy)
     for cp in st_copies():
@@ -367,41 +458,46 @@
     project(act, wb3, C, y)
     rs_core(1, y).start()
     rs_push(1)
+    for g in range(G):
+        drain(g)
     rs_finish(1, 0, 1.0, 1, second_gain, xc)
-    ag_start(1, xc)
-    ag_pass(1, xc)
+    ag_own(1, xc)
     gate_up(xc, y)
     for s in range(2):
         rs_core(1, s).wait_send()
-    ag_wait(1, 2, xc, oy, orows)
+    ag_pass(1, xc, 0, K)
+    ag_other(1, xc)
     gate_up(xc, oy)
-    project(hid, wb1, H, oy)
-    rs_core(2, oy).start()
-    project(hid, wb1, H, y)
-    rs_core(2, y).start()
-    rs_push(2)
-    rs_finish(2, 1, 0.5, 0, None, None)
-    out_local = pltpu.make_async_copy(res.at[2], out.at[crows], out_sem.at[0])
-    out_local.start()
-    out_core = rcopy(res.at[2], out.at[crows], tok_sem.at[2], out_sem.at[1], dc)
-    out_core.start()
-    for g in range(G):
-        drain(g)
+    step = F // COLS
+    for q in range(COLS):
+        project(hid, wb1, H, oy, q * step, (q + 1) * step)
+        fc_copy(oy, q).start()
+        if q:
+            last_push(q - 1)
+    for q in range(COLS):
+        project(hid, wb1, H, y, q * step, (q + 1) * step)
+        fc_copy(y, q).start()
+        if q == 0:
+            last_push(COLS - 1)
     tok_y.wait_send()
     for j in range(1, F):
-        rcopy(sc_in, scl.at[f], s_send.at[j], s_recv.at[f], dy).wait_send()
-    for s in range(2):
-        rs_core(2, s).wait_send()
-    for u in range(3):
-        rs_pair(u).wait_send()
+        rcopy(sc, scl.at[f], s_send.at[j], s_recv.at[f], dy).wait_send()
     for u, buf in enumerate((xb, xc)):
-        ag_core(u, buf).wait_send()
-        ag_pair(u, buf).wait_send()
-        ag_relay(u, buf).wait_send()
-    out_local.wait()
-    out_core.wait_send()
-    b = out.at[orows]
-    rcopy(b, b, tok_sem.at[2], out_sem.at[1], dc).wait_recv()
+        for k in range(K):
+            rs_pair(u, k).wait_send()
+            for kind in range(3):
+                ag_copy(u, kind, k, buf).wait_send()
+    for q in range(COLS):
+        last_finish(q)
+    for q in range(COLS):
+        for s in range(2):
+            fc_copy(s, q).wait_send()
+        fy_copy(q).wait_send()
+        near, far = out_copies(q)
+        near.wait()
+        far.wait_send()
+        b = out.at[orows, pl.ds(q * DC, DC)]
+        rcopy(b, b, oc_send.at[q], oc_recv.at[q], dc).wait_recv()
 
 
 def local_fused(tokens, gate_weight, up_weight, down_weight, value_weight, glu_weight, out_weight, gate_scale, up_scale,
@@ -413,26 +509,10 @@
     KW = conv_kernel.shape[0]
     RX = R // 2
     SH = S // 2
-    y = lax.rem(lax.axis_index("fs"), 2)
-
-    def part(array, side, dim):
-        width = array.shape[dim] // 2
-        return lax.dynamic_slice_in_dim(array, side * width, width, dim)
-
-    def pack(side, *weights):
-        cut = [part(w, side, 1).astype(jnp.bfloat16) for w in weights]
-        whole = cut[0] if len(cut) == 1 else jnp.concatenate(cut, axis=1)
-        return whole.reshape(2, RX, whole.shape[1])
-
-    groups = ((gate_weight, up_weight), (down_weight,), (value_weight, glu_weight), (out_weight,))
-    mine = [pack(y, *g) for g in groups]
-    theirs = [pack(1 - y, *g) for g in groups]
-    scales = jnp.zeros((8, R), jnp.float32).at[0].set(down_scale).at[1].set(out_scale)
-    rows = [v.reshape(1, -1) for v in (first_gain, conv_gain, second_gain)]
-    rows += [part(v, y, 0).reshape(1, -1) for v in (gate_scale, up_scale, value_scale, glu_scale, norm_gain)]
-    taps = part(conv_kernel, y, 1)
-    widths = [m.shape[2] for m in mine]
-    G = len(groups)
+    vectors = (down_scale, out_scale, first_gain, conv_gain, second_gain, gate_scale, up_scale, value_scale, glu_scale, norm_gain)
+    rows = [v.reshape(1, -1) for v in vectors]
+    widths = (2 * H, H, 2 * C, C)
+    G, K, NS = len(widths), SH // CHUNK, max(SUBS)
     bf, f32 = jnp.bfloat16, jnp.float32
     dma = pltpu.SemaphoreType.DMA
     anyspace = pl.BlockSpec(memory_space=pl.ANY)
@@ -441,21 +521,25 @@
     return pl.pallas_call(
         functools.partial(fused_kernel, (S, D, H, C, KW, F, RX)),
         out_shape=jax.ShapeDtypeStruct((S, D), bf),
-        in_specs=[anyspace] * (2 + 2 * G) + [vmem] * 9,
+        in_specs=[anyspace] * 7 + [vmem] * 11,
         out_specs=anyspace,
         scratch_shapes=[pltpu.VMEM((2 * F, RX, w), bf) for w in widths]
+        + [pltpu.VMEM((2, RX, w), bf) for w in widths]
+        + [pltpu.VMEM((2, R, 2 * H), f32)]
         + [pltpu.VMEM((2, S, D), bf)] * 4
         + [pltpu.VMEM((2, S, H), bf), pltpu.VMEM((2, S, D), bf)]
         + [pltpu.VMEM((3, 2, SH, D), bf), pltpu.VMEM((3, SH, D), bf), pltpu.VMEM((3, SH, D), bf), pltpu.VMEM((3, SH, D), bf)]
         + [pltpu.VMEM((2, S + pad, C), f32), pltpu.VMEM((2, S, C), f32), pltpu.VMEM((2, S, C), bf)]
-        + [pltpu.VMEM((4, 2, 8, S), f32), pltpu.VMEM((F, 8, R), f32), pltpu.VMEM((8, D), f32)]
-        + [dma((G,)), dma((G, 2)), dma((G, 2)), dma((G, F)), dma((G, F)), dma((G, F)), dma((G, F)), dma((G, F))]
-        + [dma((3,)), dma((F,)), dma((F,))]
-        + [dma((3, 2)), dma((3, 2)), dma((3,)), dma((3,)), dma((2, 3)), dma((2, 3)), dma((3,)), dma((3,)), dma((4,))],
+        + [pltpu.VMEM((4, 2, 8, S), f32), pltpu.VMEM((8, R), f32), pltpu.VMEM((F, 8, R), f32), pltpu.VMEM((8, D), f32)]
+        + [dma((2, 2)), dma((G, 2, NS)), dma((G, 2, NS))] + [dma((G, F, NS))] * 5
+        + [dma((2,)), dma((F,)), dma((F,))]
+        + [dma((3, 2)), dma((3, 2)), dma((2, K)), dma((2, K)), dma((2, 3, K)), dma((2, 3, K))]
+        + [dma((2, COLS)), dma((2, COLS)), dma((COLS,)), dma((COLS,))]
+        + [dma((3,)), dma((3,)), dma((COLS,)), dma((COLS,)), dma((COLS,))],
         compiler_params=pltpu.CompilerParams(
             collective_id=0, has_side_effects=True, vmem_limit_bytes=64 * 1024 * 1024 - 65536
         ),
-    )(tokens, *mine, *theirs, scales, *rows, taps)
+    )(tokens, gate_weight, up_weight, down_weight, value_weight, glu_weight, out_weight, *rows, conv_kernel)
 
 
 def rms_rows(rows, gains):

time: 307 us -> 279 us (0.909)
  local copies, waits for them, and re-layouts: 17.9 us -> 5.14 us
  Pallas kernels: 285 us -> 273 us
  other arithmetic: 4.02 us -> 0 us
    pallas_call x1, Pallas kernels: 285 us -> 273 us  [local_fused(): pl.pallas_call(functools.partial(fused_kernel, (S, D, H, C, KW, F, RX)),...]
    dynamic_slice x6 -> x0, local copies, waits for them, and re-layouts: 7.05 us -> none  [part(): return lax.dynamic_slice_in_dim(array, side * width, width, dim)]
    convert_element_type x4 -> x0, local copies, waits for them, and re-layouts: 5.58 us -> none  [pack(): cut = [part(w, side, 1).astype(jnp.bfloat16) for w in weights]]
    concatenate x4 -> x0, other arithmetic: 4.02 us -> none  [pack(): whole = cut[0] if len(cut) == 1 else jnp.concatenate(cut, axis=1)]
where the time goes in v2:
time: 279 us; the launch traced here: 278 us
  Pallas kernels  273 us (98%)
  local copies, waits for them, and re-layouts  5.14 us (2%)
    pallas_call x1, Pallas kernels, local_fused(): pl.pallas_call(functools.partial(fused_kernel, (S, D, H, C, KW, F, RX)),...  273 us

profile of v2, /device:TPU:0, one launch (start us, length us, event | category | flops | bytes accessed | tf_op | source)
XLA Modules:
  0.0 278.5 jit_solution(18373654317755894278)
XLA Ops:
  0.0 1.3 reshape.35.refs_12_
  1.3 1.3 reshape.36.refs_13_
  2.6 273.3 %shard_map.172 = bf16[320,2048]{1,0:T(8,128)(2,1)} custom-call(bf16[320,2048]{1,0:T(8,128)(2,1)} %refs_0_.1, f32[256,2560]{1,0:T(8,128)} %refs_1_.1, f32[256,2560]{1,0:T(8,128)} %refs_2_.1, f32[256,2560]{1,0:T(8,128)} %refs_3_.1, f32[256,1024]{1,0:T(8,128)} %refs_4_.1, f32[256,1024]{1,0:T(8,128)} %refs_5_.1, f32[256,1024]{1,0:T(8,128)} %refs_6_.1, ...), custom_call_target="tpu_custom_call" | custom-call | tf_op jit(solution)/shard_map/pallas_call | solution.py:521
  276.0 2.5 copy.20

commit v3 on v2

--- a/solution.py
+++ b/solution.py
@@ -13,7 +13,8 @@
 TILE = 256
 ROWS = 16
 CHUNK = 32
-SUBS = (1, 1, 1, 1)
+SUBS = (2, 1, 1, 1)
+VIA_X = ((0, 1), (0, 2), (0, 3))
 COLS = 4
 NT = (((1,), (1,)), ((), ()))
 TN = (((0,), (0,)), ((), ()))
@@ -29,7 +30,7 @@
     (tokens, gate_w, up_w, down_w, value_w, glu_w, out_w, down_scale, out_scale, first_gain, conv_gain, second_gain,
      gate_scale, up_scale, value_scale, glu_scale, norm_gain, conv_k, out, *scratch) = refs
     (wb0, wb1, wb2, wb3, t0, t1, t2, t3, sg, tokv, xa, xb, xc, hid, part, rc, ry, ys, res, gp, mixed, act, st, sc, scl, dsc,
-     f_sem, y_send, y_recv, u_send, d_send, z_recv, x_send, x_recv, tok_sem, s_send, s_recv,
+     f_sem, y_send, y_recv, u_send, d_send, t_send, z_recv, x_send, x_recv, tok_sem, s_send, s_recv,
      rc_send, rc_recv, ry_send, ry_recv, ag_send, ag_recv, fc_send, fc_recv, fy_send, fy_recv,
      st_send, st_recv, out_sem, oc_send, oc_recv) = scratch
     theirs, wb = (t0, t1, t2, t3), (wb0, wb1, wb2, wb3)
@@ -42,8 +43,12 @@
     z = lax.div(f, 2)
     fp = f + 1 - 2 * y
     ox, oy, oc = 1 - x, 1 - y, 1 - c
+    a = lax.rem(z, 2)
+    oa = 1 - a
     dx, dc, dy, dyc = {"rep": ox}, {"tp": oc}, {"fs": fp}, {"fs": fp, "tp": oc}
+    dz = {"fs": f + 2 - 4 * a}
     up, dn = {"fs": f + 2}, {"fs": f - 2}
+    up2, dn2 = {"fs": f + 4}, {"fs": f - 4}
 
     def rcopy(src, dst, ssem, rsem, dev):
         return pltpu.make_async_remote_copy(
@@ -60,20 +65,22 @@
 
     def round_rows(g, off, slot, ref, width, k):
         h = (x, ox)[k]
+        side = a if g < 2 else y
         fetch(slot, ref, 2 * width, h, k).wait()
 
         @pl.loop(0, RX // ROWS)
         def _(i):
             rows = pl.ds(h * RX + i * ROWS, ROWS)
             r = pl.ds(i * ROWS, ROWS)
-            near = sg[slot, rows, pl.ds(pl.multiple_of(y * width, LANES), width)]
-            far = sg[slot, rows, pl.ds(pl.multiple_of(oy * width, LANES), width)]
-            theirs[g][h, r, off:off + width] = far.astype(jnp.bfloat16)
+            near = sg[slot, rows, pl.ds(pl.multiple_of(side * width, LANES), width)]
             wb[g][2 * f + h, r, off:off + width] = near.astype(jnp.bfloat16)
+            if g >= 2 or k == 0:
+                far = sg[slot, rows, pl.ds(pl.multiple_of((1 - side) * width, LANES), width)]
+                theirs[g][h if g >= 2 else 0, r, off:off + width] = far.astype(jnp.bfloat16)
 
     fetch_start(0, gate_w, 2 * H)
     fetch_start(1, up_w, 2 * H)
-    tok_local = pltpu.make_async_copy(tokens, tokv.at[y], out_sem.at[0])
+    tok_local = pltpu.make_async_copy(tokens, tokv.at[a], out_sem.at[0])
     tok_local.start()
     sc[...] = jnp.zeros_like(sc)
     sc[0:1, :] = down_scale[...]
@@ -91,7 +98,7 @@
         return ref.at[lead, pl.ds(i * n, n)]
 
     def y_copy(g, h, k, i):
-        return rcopy(piece(g, theirs[g], h, i), piece(g, wb[g], 2 * f + h, i), y_send.at[g, k, i], y_recv.at[g, k, i], dy)
+        return rcopy(piece(g, theirs[g], h, i), piece(g, wb[g], 2 * f + h, i), y_send.at[g, 0, k, i], y_recv.at[g, 0, k, i], dy)
 
     def y_start(g, k):
         for i in range(SUBS[g]):
@@ -99,7 +106,7 @@
 
     def y_wait(g, h, k, i):
         b = piece(g, wb[g], 2 * fp + h, i)
-        rcopy(b, b, y_send.at[g, k, i], y_recv.at[g, k, i], dy).wait_recv()
+        rcopy(b, b, y_send.at[g, 0, k, i], y_recv.at[g, 0, k, i], dy).wait_recv()
 
     def z_copy(g, q, i, sems, dev):
         b = piece(g, wb[g], 2 * q + x, i)
@@ -184,31 +191,162 @@
                 for i in range(SUBS[g]):
                     x_copy(g, q, i).wait_send()
 
+    def ff_own(g):
+        for i in range(SUBS[g]):
+            b = piece(g, wb[g], 2 * f + x, i)
+            t = piece(g, theirs[g], 0, i)
+
+            @pl.when(z > 0)
+            def _():
+                rcopy(t, b, t_send.at[g, 0, i], z_recv.at[g, f, i], dn).start()
+
+            @pl.when(z < Z - 1)
+            def _():
+                rcopy(t, b, t_send.at[g, 1, i], z_recv.at[g, f, i], up).start()
+
+            @pl.when(z >= 2)
+            def _():
+                z_copy(g, f, i, d_send, dn2).start()
+
+            @pl.when(z < Z - 2)
+            def _():
+                z_copy(g, f, i, u_send, up2).start()
+
+    def ff_y(g, zq, k, i):
+        b = piece(g, wb[g], 2 * (2 * zq + y) + (x, ox)[k], i)
+        return rcopy(b, b, y_send.at[g, zq, k, i], y_recv.at[g, zq, k, i], dy)
+
+    def ff_y_own(g, k):
+        for i in range(SUBS[g]):
+            ff_y(g, z, k, i).start()
+
+    def ff_y_wait(g, zq, k, i):
+        b = piece(g, wb[g], 2 * (2 * zq + oy) + (x, ox)[k], i)
+        rcopy(b, b, y_send.at[g, zq, k, i], y_recv.at[g, zq, k, i], dy).wait_recv()
+
+    def ff_x_wait(g, q, i):
+        b = piece(g, wb[g], 2 * q + ox, i)
+        rcopy(b, b, x_send.at[g, q, i], x_recv.at[g, q, i], dx).wait_recv()
+
+    def both_sides(g, d, act_on):
+        for i in range(SUBS[g]):
+            @pl.when(z >= d)
+            def _():
+                act_on(z - d, -1, i)
+
+            @pl.when(z + d < Z)
+            def _():
+                act_on(z + d, 1, i)
+
+    def ff_arrive(g, d):
+        def act_on(zq, side, i):
+            q = 2 * zq + y
+            z_copy(g, q, i, u_send, up).wait_recv()
+            if side < 0:
+                @pl.when(z < Z - 2)
+                def _():
+                    z_copy(g, q, i, u_send, up2).start()
+            else:
+                @pl.when(z >= 2)
+                def _():
+                    z_copy(g, q, i, d_send, dn2).start()
+            x_copy(g, q, i).start()
+            ff_y(g, zq, 0, i).start()
+
+        both_sides(g, d, act_on)
+
+    def ff_relay(g, d):
+        def act_on(zq, side, i):
+            if (g, d) in VIA_X:
+                ff_y_wait(g, zq, 0, i)
+                x_copy(g, 2 * zq + oy, i).start()
+            else:
+                ff_x_wait(g, 2 * zq + y, i)
+                ff_y(g, zq, 1, i).start()
+
+        both_sides(g, d, act_on)
+
+    def ff_done(g):
+        for i in range(SUBS[g]):
+            for k in range(2):
+                ff_y_wait(g, z, k, i)
+        for d in range(1, Z):
+            def act_on(zq, side, i):
+                if (g, d) in VIA_X:
+                    ff_x_wait(g, 2 * zq + y, i)
+                    ff_x_wait(g, 2 * zq + oy, i)
+                else:
+                    ff_y_wait(g, zq, 0, i)
+                    ff_y_wait(g, zq, 1, i)
+
+            both_sides(g, d, act_on)
+
+    def ff_drain(g):
+        for i in range(SUBS[g]):
+            b = piece(g, wb[g], 2 * f + x, i)
+            t = piece(g, theirs[g], 0, i)
+
+            @pl.when(z > 0)
+            def _():
+                rcopy(t, b, t_send.at[g, 0, i], z_recv.at[g, f, i], dn).wait_send()
+
+            @pl.when(z < Z - 1)
+            def _():
+                rcopy(t, b, t_send.at[g, 1, i], z_recv.at[g, f, i], up).wait_send()
+
+            @pl.when(z >= 2)
+            def _():
+                z_copy(g, f, i, d_send, dn2).wait_send()
+
+            @pl.when(z < Z - 2)
+            def _():
+                z_copy(g, f, i, u_send, up2).wait_send()
+
+            for k in range(2):
+                ff_y(g, z, k, i).wait_send()
+        for d in range(1, Z):
+            def act_on(zq, side, i):
+                q = 2 * zq + y
+                if side < 0:
+                    @pl.when(z < Z - 2)
+                    def _():
+                        z_copy(g, q, i, u_send, up2).wait_send()
+                else:
+                    @pl.when(z >= 2)
+                    def _():
+                        z_copy(g, q, i, d_send, dn2).wait_send()
+                x_copy(g, q, i).wait_send()
+                ff_y(g, zq, 0, i).wait_send()
+                if (g, d) in VIA_X:
+                    x_copy(g, 2 * zq + oy, i).wait_send()
+                else:
+                    ff_y(g, zq, 1, i).wait_send()
+
+            both_sides(g, d, act_on)
+
+    crows = pl.ds(c * SH, SH)
+    orows = pl.ds(oc * SH, SH)
+    tok_z = rcopy(tokens.at[crows], tokv.at[a, crows], tok_sem.at[0], tok_sem.at[1], dz)
+    there = tokv.at[oa, crows]
+    tok_core = rcopy(there, there, tok_sem.at[2], tok_sem.at[3], dc)
     for k in range(2):
         round_rows(0, 0, 0, gate_w, H, k)
         round_rows(0, H, 1, up_w, H, k)
-    y_start(0, 0)
-    send_rows(0, f, False)
+    ff_own(0)
+    ff_y_own(0, 0)
     fetch_start(0, down_w, 2 * H)
     fetch_start(1, value_w, 2 * C)
+    tok_z.start()
     for k in range(2):
         round_rows(1, 0, 0, down_w, H, k)
     fetch_start(0, glu_w, 2 * C)
-    y_start(1, 0)
     for k in range(2):
         round_rows(2, 0, 1, value_w, C, k)
     fetch_start(1, out_w, 2 * C)
     for k in range(2):
         round_rows(2, C, 0, glu_w, C, k)
-    y_start(2, 0)
     for k in range(2):
         round_rows(3, 0, 1, out_w, C, k)
-    y_start(3, 0)
-    y_start(0, 1)
-    tok_y = rcopy(tokens, tokv.at[y], tok_sem.at[0], tok_sem.at[1], dy)
-    tok_y.start()
-    for g in range(1, G):
-        y_start(g, 1)
     for j in range(1, F):
         rcopy(sc, scl.at[f], s_send.at[j], s_recv.at[f], {"fs": lax.rem(f + j, F)}).start()
 
@@ -225,11 +363,11 @@
         @pl.loop(0, H // TILE)
         def _(j):
             lo = pl.multiple_of(j * TILE, TILE)
-            a = src[s]
+            rows = src[s]
             gw = wb0[:, :, pl.ds(lo, TILE)].reshape(D, TILE)
             uw = wb0[:, :, pl.ds(H + lo, TILE)].reshape(D, TILE)
-            gv = jnp.dot(a, gw, preferred_element_type=jnp.float32) * gate_scale[:, pl.ds(pl.multiple_of(y * H + lo, LANES), TILE)]
-            uv = jnp.dot(a, uw, preferred_element_type=jnp.float32) * up_scale[:, pl.ds(pl.multiple_of(y * H + lo, LANES), TILE)]
+            gv = jnp.dot(rows, gw, preferred_element_type=jnp.float32) * gate_scale[:, pl.ds(pl.multiple_of(a * H + lo, LANES), TILE)]
+            uv = jnp.dot(rows, uw, preferred_element_type=jnp.float32) * up_scale[:, pl.ds(pl.multiple_of(a * H + lo, LANES), TILE)]
             hid[s, :, pl.ds(lo, TILE)] = (gv * jax.nn.sigmoid(gv) * uv).astype(jnp.bfloat16)
 
     def project(src, w, width, s, first=0, last=F):
@@ -239,29 +377,30 @@
             p = lax.dot_general(src[s], rows, NT, preferred_element_type=jnp.float32)
             part[s, :, pl.ds(pl.multiple_of(j * R, R), R)] = p.astype(jnp.bfloat16)
 
-    crows = pl.ds(c * SH, SH)
-    orows = pl.ds(oc * SH, SH)
+    SIDES = ((a, oa, dz), (y, oy, dy), (a, oa, dz))
 
     def rs_core(u, s):
         return rcopy(part.at[s, orows], rc.at[u, s], rc_send.at[u, s], rc_recv.at[u, s], dc)
 
     def rs_pair(u, k):
         r = pl.ds(k * CHUNK, CHUNK)
-        return rcopy(ys.at[u, r], ry.at[u, r], ry_send.at[u, k], ry_recv.at[u, k], dy)
+        return rcopy(ys.at[u, r], ry.at[u, r], ry_send.at[u, k], ry_recv.at[u, k], SIDES[u][2])
 
     def rs_push(u):
-        rs_core(u, oy).wait_recv()
+        ot = SIDES[u][1]
+        rs_core(u, ot).wait_recv()
         for k in range(K):
             @pl.loop(0, CHUNK // ROWS)
             def _(i):
                 r = pl.ds(k * CHUNK + i * ROWS, ROWS)
-                p = part[oy, pl.ds(c * SH + k * CHUNK + i * ROWS, ROWS), :].astype(jnp.float32)
-                ys[u, r, :] = (p + rc[u, oy, r, :].astype(jnp.float32)).astype(jnp.bfloat16)
+                p = part[ot, pl.ds(c * SH + k * CHUNK + i * ROWS, ROWS), :].astype(jnp.float32)
+                ys[u, r, :] = (p + rc[u, ot, r, :].astype(jnp.float32)).astype(jnp.bfloat16)
 
             rs_pair(u, k).start()
 
     def rs_finish(u, base, factor, scale_row, gains, dst):
-        rs_core(u, y).wait_recv()
+        me, slot = SIDES[u][0], SIDES[u + 1][0]
+        rs_core(u, me).wait_recv()
         for k in range(K):
             rs_pair(u, k).wait_recv()
 
@@ -269,12 +408,12 @@
             def _(i):
                 r = pl.ds(k * CHUNK + i * ROWS, ROWS)
                 rr = pl.ds(c * SH + k * CHUNK + i * ROWS, ROWS)
-                total = part[y, rr, :].astype(jnp.float32) + rc[u, y, r, :].astype(jnp.float32)
+                total = part[me, rr, :].astype(jnp.float32) + rc[u, me, r, :].astype(jnp.float32)
                 total = total + ry[u, r, :].astype(jnp.float32)
-                b = tokv[y, rr, :] if base is None else res[base, r, :]
+                b = tokv[me, rr, :] if base is None else res[base, r, :]
                 now = (b.astype(jnp.float32) + dsc[scale_row:scale_row + 1, :] * factor * total).astype(jnp.bfloat16)
                 res[u, r, :] = now
-                dst[y, rr, :] = norm(now.astype(jnp.float32), gains[...])
+                dst[slot, rr, :] = norm(now.astype(jnp.float32), gains[...])
 
             ag_copy(u, 1, k, dst).start()
             ag_copy(u, 0, k, dst).start()
@@ -283,11 +422,13 @@
         return pl.ds(side * SH + k * CHUNK, CHUNK)
 
     def ag_copy(u, kind, k, buf):
-        b = buf.at[oy if kind == 2 else y, ag_rows(k, c)]
-        return rcopy(b, b, ag_send.at[u, kind, k], ag_recv.at[u, kind, k], dy if kind == 1 else dc)
+        me, ot, partner = SIDES[u + 1]
+        b = buf.at[ot if kind == 2 else me, ag_rows(k, c)]
+        return rcopy(b, b, ag_send.at[u, kind, k], ag_recv.at[u, kind, k], partner if kind == 1 else dc)
 
     def ag_wait(u, kind, k, buf):
-        b = buf.at[y if kind == 0 else oy, ag_rows(k, c if kind == 1 else oc)]
+        me, ot, _ = SIDES[u + 1]
+        b = buf.at[me if kind == 0 else ot, ag_rows(k, c if kind == 1 else oc)]
         rcopy(b, b, ag_send.at[u, kind, k], ag_recv.at[u, kind, k], dc).wait_recv()
 
     def ag_pass(u, buf, first, last):
@@ -309,17 +450,17 @@
 
     def fy_copy(q):
         cols = pl.ds(q * DC, DC)
-        return rcopy(ys.at[2, :, cols], ry.at[2, :, cols], fy_send.at[q], fy_recv.at[q], dy)
+        return rcopy(ys.at[2, :, cols], ry.at[2, :, cols], fy_send.at[q], fy_recv.at[q], dz)
 
     def last_push(q):
         cols = pl.ds(q * DC, DC)
-        fc_copy(oy, q).wait_recv()
+        fc_copy(oa, q).wait_recv()
 
         @pl.loop(0, SH // ROWS)
         def _(i):
             r = pl.ds(i * ROWS, ROWS)
-            p = part[oy, pl.ds(c * SH + i * ROWS, ROWS), cols].astype(jnp.float32)
-            ys[2, r, cols] = (p + rc[2, oy, r, cols].astype(jnp.float32)).astype(jnp.bfloat16)
+            p = part[oa, pl.ds(c * SH + i * ROWS, ROWS), cols].astype(jnp.float32)
+            ys[2, r, cols] = (p + rc[2, oa, r, cols].astype(jnp.float32)).astype(jnp.bfloat16)
 
         fy_copy(q).start()
 
@@ -330,13 +471,13 @@
 
     def last_finish(q):
         cols = pl.ds(q * DC, DC)
-        fc_copy(y, q).wait_recv()
+        fc_copy(a, q).wait_recv()
         fy_copy(q).wait_recv()
 
         @pl.loop(0, SH // ROWS)
         def _(i):
             r = pl.ds(i * ROWS, ROWS)
-            total = part[y, pl.ds(c * SH + i * ROWS, ROWS), cols].astype(jnp.float32) + rc[2, y, r, cols].astype(jnp.float32)
+            total = part[a, pl.ds(c * SH + i * ROWS, ROWS), cols].astype(jnp.float32) + rc[2, a, r, cols].astype(jnp.float32)
             total = total + ry[2, r, cols].astype(jnp.float32)
             res[2, r, cols] = (res[1, r, cols].astype(jnp.float32) + 0.5 * dsc[0:1, cols] * total).astype(jnp.bfloat16)
 
@@ -347,11 +488,11 @@
         @pl.loop(0, C // TILE)
         def _(j):
             lo = pl.multiple_of(j * TILE, TILE)
-            a = xb[s]
+            rows = xb[s]
             vw = wb2[:, :, pl.ds(lo, TILE)].reshape(D, TILE)
             gw = wb2[:, :, pl.ds(C + lo, TILE)].reshape(D, TILE)
-            vv = jnp.dot(a, vw, preferred_element_type=jnp.float32) * value_scale[:, pl.ds(pl.multiple_of(y * C + lo, LANES), TILE)]
-            gv = jnp.dot(a, gw, preferred_element_type=jnp.float32) * glu_scale[:, pl.ds(pl.multiple_of(y * C + lo, LANES), TILE)]
+            vv = jnp.dot(rows, vw, preferred_element_type=jnp.float32) * value_scale[:, pl.ds(pl.multiple_of(y * C + lo, LANES), TILE)]
+            gv = jnp.dot(rows, gw, preferred_element_type=jnp.float32) * glu_scale[:, pl.ds(pl.multiple_of(y * C + lo, LANES), TILE)]
             g = (vv * jax.nn.sigmoid(gv)).astype(jnp.bfloat16)
             gp[s, pl.ds(PAD, S), pl.ds(lo, TILE)] = g.astype(jnp.float32)
 
@@ -393,34 +534,57 @@
             v = (mixed[s, :, cols] - mcol) * rcol * norm_gain[:, pl.ds(pl.multiple_of(y * C + j * LANES, LANES), LANES)]
             act[s, :, cols] = (v * jax.nn.sigmoid(v)).astype(jnp.bfloat16)
 
-    def own_and_pair(g):
-        send_rows(g, f, False)
-        send_rows(g, fp, True)
-
-    send_rows(0, fp, True)
     tok_local.wait()
-    norm_tokens(y)
-    forward(0, 1)
-    for d in range(2, Z - 1):
-        forward(0, d)
-    own_and_pair(1)
-    tok_y.wait_recv()
-    norm_tokens(oy)
-    forward(0, Z - 1)
-    forward(1, 1)
-    group_done(0)
-    gate_up(xa, oy)
-    for d in range(2, Z - 1):
-        forward(1, d)
-    own_and_pair(2)
-    gate_up(xa, y)
-    forward(1, Z - 1)
+    norm_tokens(a)
+    ff_arrive(0, 1)
+    ff_y_own(0, 1)
+    ff_own(1)
+    ff_arrive(0, 2)
+    ff_relay(0, 1)
+    for d in range(3, Z):
+        ff_arrive(0, d)
+    y_start(2, 0)
+    y_start(3, 0)
+    ff_y_own(1, 0)
+    ff_arrive(1, 1)
+    ff_relay(0, 2)
+    rcopy(there, there, tok_sem.at[0], tok_sem.at[1], dz).wait_recv()
+    tok_core.start()
+    send_rows(2, f, False)
+    send_rows(3, f, False)
+    send_rows(2, fp, True)
+    send_rows(3, fp, True)
+    ff_arrive(1, 2)
+    for d in range(3, Z):
+        ff_arrive(1, d)
+    ff_y_own(1, 1)
+    for d in range(3, Z):
+        ff_relay(0, d)
+    b = tokv.at[oa, orows]
+    rcopy(b, b, tok_sem.at[2], tok_sem.at[3], dc).wait_recv()
+    norm_tokens(oa)
     forward(2, 1)
-    group_done(1)
-    project(hid, wb1, H, oy)
-    rs_core(0, oy).start()
-    project(hid, wb1, H, y)
-    rs_core(0, y).start()
+    forward(2, 2)
+    ff_relay(1, 1)
+    ff_relay(1, 2)
+    for d in range(3, Z):
+        forward(2, d)
+    for d in range(3, Z):
+        ff_relay(1, d)
+    forward(3, 1)
+    forward(3, 2)
+    ff_done(0)
+    gate_up(xa, oa)
+    for d in range(3, Z):
+        forward(3, d)
+    gate_up(xa, a)
+    ff_done(1)
+    y_start(2, 1)
+    y_start(3, 1)
+    project(hid, wb1, H, oa)
+    rs_core(0, oa).start()
+    project(hid, wb1, H, a)
+    rs_core(0, a).start()
     rs_push(0)
     for j in range(1, F):
         b = scl.at[lax.rem(f + j, F)]
@@ -428,14 +592,7 @@
     scl[f] = sc[...]
     for j in range(F):
         dsc[:, j * R:(j + 1) * R] = scl[j]
-    for d in range(2, Z - 1):
-        forward(2, d)
-    own_and_pair(3)
-    forward(2, Z - 1)
-    forward(3, 1)
     rs_finish(0, None, 0.5, 0, conv_gain, xb)
-    for d in range(2, Z):
-        forward(3, d)
     ag_pass(0, xb, 0, K)
     ag_own(0, xb)
     group_done(2)
@@ -458,28 +615,31 @@
     project(act, wb3, C, y)
     rs_core(1, y).start()
     rs_push(1)
-    for g in range(G):
+    for g in (0, 1):
+        ff_drain(g)
+    for g in (2, 3):
         drain(g)
     rs_finish(1, 0, 1.0, 1, second_gain, xc)
     ag_own(1, xc)
-    gate_up(xc, y)
+    gate_up(xc, a)
     for s in range(2):
         rs_core(1, s).wait_send()
     ag_pass(1, xc, 0, K)
     ag_other(1, xc)
-    gate_up(xc, oy)
+    gate_up(xc, oa)
     step = F // COLS
     for q in range(COLS):
-        project(hid, wb1, H, oy, q * step, (q + 1) * step)
-        fc_copy(oy, q).start()
+        project(hid, wb1, H, oa, q * step, (q + 1) * step)
+        fc_copy(oa, q).start()
         if q:
             last_push(q - 1)
     for q in range(COLS):
-        project(hid, wb1, H, y, q * step, (q + 1) * step)
-        fc_copy(y, q).start()
+        project(hid, wb1, H, a, q * step, (q + 1) * step)
+        fc_copy(a, q).start()
         if q == 0:
             last_push(COLS - 1)
-    tok_y.wait_send()
+    tok_z.wait_send()
+    tok_core.wait_send()
     for j in range(1, F):
         rcopy(sc, scl.at[f], s_send.at[j], s_recv.at[f], dy).wait_send()
     for u, buf in enumerate((xb, xc)):
@@ -524,15 +684,15 @@
         in_specs=[anyspace] * 7 + [vmem] * 11,
         out_specs=anyspace,
         scratch_shapes=[pltpu.VMEM((2 * F, RX, w), bf) for w in widths]
-        + [pltpu.VMEM((2, RX, w), bf) for w in widths]
+        + [pltpu.VMEM((1 if g < 2 else 2, RX, w), bf) for g, w in enumerate(widths)]
         + [pltpu.VMEM((2, R, 2 * H), f32)]
         + [pltpu.VMEM((2, S, D), bf)] * 4
         + [pltpu.VMEM((2, S, H), bf), pltpu.VMEM((2, S, D), bf)]
         + [pltpu.VMEM((3, 2, SH, D), bf), pltpu.VMEM((3, SH, D), bf), pltpu.VMEM((3, SH, D), bf), pltpu.VMEM((3, SH, D), bf)]
         + [pltpu.VMEM((2, S + pad, C), f32), pltpu.VMEM((2, S, C), f32), pltpu.VMEM((2, S, C), bf)]
         + [pltpu.VMEM((4, 2, 8, S), f32), pltpu.VMEM((8, R), f32), pltpu.VMEM((F, 8, R), f32), pltpu.VMEM((8, D), f32)]
-        + [dma((2, 2)), dma((G, 2, NS)), dma((G, 2, NS))] + [dma((G, F, NS))] * 5
-        + [dma((2,)), dma((F,)), dma((F,))]
+        + [dma((2, 2)), dma((G, F // 2, 2, NS)), dma((G, F // 2, 2, NS))] + [dma((G, F, NS))] * 2 + [dma((2, 2, NS))] + [dma((G, F, NS))] * 3
+        + [dma((4,)), dma((F,)), dma((F,))]
         + [dma((3, 2)), dma((3, 2)), dma((2, K)), dma((2, K)), dma((2, 3, K)), dma((2, 3, K))]
         + [dma((2, COLS)), dma((2, COLS)), dma((COLS,)), dma((COLS,))]
         + [dma((3,)), dma((3,)), dma((COLS,)), dma((COLS,)), dma((COLS,))],
@@ -711,7 +871,7 @@
 
 
 def fits(mesh):
-    return mesh.shape["rep"] == 2 and mesh.shape["tp"] == 2 and mesh.shape["fs"] % 2 == 0 and mesh.shape["fs"] >= 4
+    return mesh.shape["rep"] == 2 and mesh.shape["tp"] == 2 and mesh.shape["fs"] % 4 == 0
 
 
 def solution(mesh):

time: 279 us -> 259 us (0.928)
  Pallas kernels: 273 us -> 253 us
    pallas_call x1, Pallas kernels: 273 us -> 253 us  [local_fused(): pl.pallas_call(functools.partial(fused_kernel, (S, D, H, C, KW, F, RX)),...]
where the time goes in v3:
time: 259 us; the launch traced here: 258 us
  Pallas kernels  253 us (98%)
  local copies, waits for them, and re-layouts  5.14 us (2%)
    pallas_call x1, Pallas kernels, local_fused(): pl.pallas_call(functools.partial(fused_kernel, (S, D, H, C, KW, F, RX)),...  253 us

profile of v3, /device:TPU:0, one launch (start us, length us, event | category | flops | bytes accessed | tf_op | source)
XLA Modules:
  0.0 258.2 jit_solution(6309926069872942894)
XLA Ops:
  0.0 1.3 reshape.35.refs_12_
  1.3 1.3 reshape.36.refs_13_
  2.6 253.1 %shard_map.172 = bf16[320,2048]{1,0:T(8,128)(2,1)} custom-call(bf16[320,2048]{1,0:T(8,128)(2,1)} %refs_0_.1, f32[256,2560]{1,0:T(8,128)} %refs_1_.1, f32[256,2560]{1,0:T(8,128)} %refs_2_.1, f32[256,2560]{1,0:T(8,128)} %refs_3_.1, f32[256,1024]{1,0:T(8,128)} %refs_4_.1, f32[256,1024]{1,0:T(8,128)} %refs_5_.1, f32[256,1024]{1,0:T(8,128)} %refs_6_.1, ...), custom_call_target="tpu_custom_call" | custom-call | tf_op jit(solution)/shard_map/pallas_call | solution.py:681
  255.7 2.5 copy.20

commit v4 on v3

--- a/solution.py
+++ b/solution.py
@@ -359,6 +359,10 @@
             r = pl.ds(i * ROWS, ROWS)
             xa[s, r, :] = norm(tokv[s, r, :].astype(jnp.float32), first_gain[...])
 
+    def wide(ref, j):
+        first, n = a * (H // LANES) + j * (TILE // LANES), TILE // LANES
+        return jnp.concatenate([ref[pl.ds(first + t, 1), :] for t in range(n)], axis=1)
+
     def gate_up(src, s):
         @pl.loop(0, H // TILE)
         def _(j):
@@ -366,8 +370,8 @@
             rows = src[s]
             gw = wb0[:, :, pl.ds(lo, TILE)].reshape(D, TILE)
             uw = wb0[:, :, pl.ds(H + lo, TILE)].reshape(D, TILE)
-            gv = jnp.dot(rows, gw, preferred_element_type=jnp.float32) * gate_scale[:, pl.ds(pl.multiple_of(a * H + lo, LANES), TILE)]
-            uv = jnp.dot(rows, uw, preferred_element_type=jnp.float32) * up_scale[:, pl.ds(pl.multiple_of(a * H + lo, LANES), TILE)]
+            gv = jnp.dot(rows, gw, preferred_element_type=jnp.float32) * wide(gate_scale, j)
+            uv = jnp.dot(rows, uw, preferred_element_type=jnp.float32) * wide(up_scale, j)
             hid[s, :, pl.ds(lo, TILE)] = (gv * jax.nn.sigmoid(gv) * uv).astype(jnp.bfloat16)
 
     def project(src, w, width, s, first=0, last=F):
@@ -670,7 +674,7 @@
     RX = R // 2
     SH = S // 2
     vectors = (down_scale, out_scale, first_gain, conv_gain, second_gain, gate_scale, up_scale, value_scale, glu_scale, norm_gain)
-    rows = [v.reshape(1, -1) for v in vectors]
+    rows = [v.reshape(-1, LANES) if v is gate_scale or v is up_scale else v.reshape(1, -1) for v in vectors]
     widths = (2 * H, H, 2 * C, C)
     G, K, NS = len(widths), SH // CHUNK, max(SUBS)
     bf, f32 = jnp.bfloat16, jnp.float32

time: 259 us -> 256 us (0.988)
  local copies, waits for them, and re-layouts: 5.14 us -> 2.52 us
    reshape x2 -> x0, local copies, waits for them, and re-layouts: 2.62 us -> none  [local_fused(): rows = [v.reshape(1, -1) for v in vectors]]
where the time goes in v4:
time: 256 us
  Pallas kernels  253 us (99%)
    pallas_call x1, Pallas kernels, local_fused(): pl.pallas_call(functools.partial(fused_kernel, (S, D, H, C, KW, F, RX)),...  253 us

profile of v4, /device:TPU:0, one launch (start us, length us, event | category | flops | bytes accessed | tf_op | source)
XLA Modules:
  0.0 255.6 jit_solution(12990417049335885878)
XLA Ops:
  0.0 253.1 %shard_map.172 = bf16[320,2048]{1,0:T(8,128)(2,1)} custom-call(bf16[320,2048]{1,0:T(8,128)(2,1)} %refs_0_.1, f32[256,2560]{1,0:T(8,128)} %refs_1_.1, f32[256,2560]{1,0:T(8,128)} %refs_2_.1, f32[256,2560]{1,0:T(8,128)} %refs_3_.1, f32[256,1024]{1,0:T(8,128)} %refs_4_.1, f32[256,1024]{1,0:T(8,128)} %refs_5_.1, f32[256,1024]{1,0:T(8,128)} %refs_6_.1, ...), custom_call_target="tpu_custom_call" | custom-call | tf_op jit(solution)/shard_map/pallas_call | solution.py:685
  253.1 2.5 copy.20
